TPU v7x, 256 devices: a whole 4x4x8 slice. The times are simulated.
256 devices in a mesh: sp: 64 (over z, y, core), tp: 4 (over x).
Axes of the slice: x: 4, y: 4, z: 8, core: 2. Of those that a mesh axis runs over, the one named last changes fastest.
Arguments:
- queries: bfloat16 [16384, 2048], P('sp', 'tp'), may hold values from -6 to 6
- keys: bfloat16 [16384, 512], P('sp', 'tp'), may hold values from -6 to 6
- values: bfloat16 [16384, 512], P('sp', 'tp'), may hold values from -6 to 6
- query_gain: float32 [64], replicated, may hold values from 0.8 to 5
- key_gain: float32 [64], replicated, may hold values from 0.8 to 5
- stream: bfloat16 [16384, 2048], P('sp'), may hold values from -0.1796875 to 0.1796875
- out_weight: bfloat16 [2048, 2048], P('tp'), may hold values from -0.125 to 0.125
- mixer_gain: float32 [2048], replicated, may hold values from 0.1 to 1.9
- up_weight: bfloat16 [2048, 8192], P('sp', 'tp'), may hold values from -0.125 to 0.125
- down_weight: bfloat16 [8192, 2048], P('tp', 'sp'), may hold values from -0.0625 to 0.0625
Outputs:
- updated: bfloat16 [16384, 2048], P('sp', 'tp')
All inputs are finite; a program needn't handle non-finite values.
Results may differ from a plain program's by a relative error of at most 0.02.
The roundings to bfloat16 on the way count: a program that leaves them out, or rounds other values in their place, can miss the bound.
Values may be sent and summed in bfloat16 or wider, within the bound.
A program may use at most 128 MiB of HBM per device.

v0:
```python
import math

import jax
import jax.numpy as jnp
from jax import lax
from jax.sharding import PartitionSpec as P

HD = 64
GRID_W = 64


EPSILON = 1e-06


def turned_gather(arrays, axis, dims):
    turned = [jnp.moveaxis(a, dim, 0) for a, dim in zip(arrays, dims)]
    widths = [t[0].size for t in turned]
    both = jnp.concatenate([t.reshape(-1, w) for t, w in zip(turned, widths)], axis=1)
    filled = lax.all_gather(both, axis, axis=0, tiled=True)
    pieces = jnp.split(filled, [sum(widths[:k]) for k in range(1, len(widths))], axis=1)
    return tuple(
        (
            jnp.moveaxis(b.reshape(-1, *t.shape[1:]), 0, dim)
            for b, t, dim in zip(pieces, turned, dims)
        )
    )


def sent_together(arrays, axis, dim, along):
    ends, at = ([], 0)
    for a in arrays[:-1]:
        at += a.shape[along]
        ends.append(at)
    both = jnp.concatenate(arrays, axis=along)
    return tuple(jnp.split(lax.all_gather(both, axis, axis=dim, tiled=True), ends, axis=along))


def in_blocks(x, dim, count):
    dims = x.shape
    pieces = x.reshape(*dims[:dim], count, dims[dim] // count, *dims[dim + 1 :])
    return jnp.moveaxis(pieces, dim, 0)


def sum_at_owner(x, axis, dim):
    pieces = in_blocks(x, dim, lax.axis_size(axis))
    arrived = lax.all_to_all(pieces, axis, split_axis=0, concat_axis=0, tiled=True)
    return arrived.astype(jnp.float32).sum(axis=0)


def laid_out(pieces, dim):
    pieces = jnp.moveaxis(pieces, 0, dim)
    dims = pieces.shape
    return pieces.reshape(*dims[:dim], dims[dim] * dims[dim + 1], *dims[dim + 2 :])


def copy_for_each(x, axis):
    copies = jnp.broadcast_to(x, (lax.axis_size(axis), *x.shape))
    return lax.all_to_all(copies, axis, split_axis=0, concat_axis=0, tiled=True)


def gather_directly(x, axis, dim):
    return laid_out(copy_for_each(x, axis), dim)


def prepare(projected, gain_vec, offset):
    row_count = projected.shape[0]
    head_count = projected.shape[1] // HD
    widened = projected.astype(jnp.float32).reshape(row_count, head_count, HD)
    widened = (
        widened
        * lax.rsqrt(jnp.mean(widened * widened, axis=-1, keepdims=True) + EPSILON)
        * gain_vec
    )
    position = offset + jnp.arange(row_count, dtype=jnp.int32)
    grid_row = (position // GRID_W).astype(jnp.float32)
    grid_col = (position % GRID_W).astype(jnp.float32)
    half_dim = HD // 2
    inverse = 1.0 / jnp.power(10000.0, jnp.arange(0, half_dim, 2, dtype=jnp.float32) / half_dim)
    angle = jnp.concatenate([grid_row[:, None] * inverse, grid_col[:, None] * inverse], axis=-1)
    cosine = jnp.cos(angle)[:, None, :]
    sine_table = jnp.sin(angle)[:, None, :]
    paired = widened.reshape(row_count, head_count, half_dim, 2)
    former = paired[..., 0]
    latter = paired[..., 1]
    rotated = jnp.stack(
        [former * cosine - latter * sine_table, former * sine_table + latter * cosine], axis=-1
    )
    return rotated.reshape(row_count, head_count, HD).astype(jnp.bfloat16)


def attend_block(state, grouped, key_block, value_block):
    running, totals, weighted = state
    scores = jnp.einsum("qhgd,khd->hgqk", grouped, key_block, preferred_element_type=jnp.float32)
    scores = scores * (1.0 / math.sqrt(HD))
    newest = jnp.maximum(running, jnp.max(scores, axis=-1))
    rescale = jnp.exp(running - newest)
    exps = jnp.exp(scores - newest[..., None])
    totals = totals * rescale + jnp.sum(exps, axis=-1)
    weighted = weighted * rescale[..., None] + jnp.einsum(
        "hgqk,khd->hgqd", exps.astype(jnp.bfloat16), value_block, preferred_element_type=jnp.float32
    )
    return (newest, totals, weighted)


def shards(
    queries,
    keys,
    values,
    query_gain,
    key_gain,
    stream,
    out_weight,
    mixer_gain,
    up_weight,
    down_weight,
):
    local_rows = queries.shape[0]
    offset = lax.axis_index("sp") * local_rows
    up_whole, down_whole = turned_gather((up_weight, down_weight), "sp", (0, 1))
    kv_count = keys.shape[1] // HD
    group_size = queries.shape[1] // HD // kv_count
    grouped = prepare(queries, query_gain, offset).reshape(local_rows, kv_count, group_size, HD)
    prepared_keys = prepare(keys, key_gain, offset).reshape(local_rows, kv_count * HD)
    initial = (
        jnp.full((kv_count, group_size, local_rows), -1e30, jnp.float32),
        jnp.zeros((kv_count, group_size, local_rows), jnp.float32),
        jnp.zeros((kv_count, group_size, local_rows, HD), jnp.float32),
    )
    key_rows, value_rows = sent_together((prepared_keys, values), "sp", 0, 1)
    piece_rows = key_rows.shape[0]
    block_rows = math.gcd(piece_rows, 2048)
    key_blocks = key_rows.reshape(piece_rows // block_rows, block_rows, kv_count, HD)
    value_blocks = value_rows.reshape(piece_rows // block_rows, block_rows, kv_count, HD)

    def visit_block(block_index, state_now):
        return attend_block(state_now, grouped, key_blocks[block_index], value_blocks[block_index])

    running, totals, weighted = lax.fori_loop(0, piece_rows // block_rows, visit_block, initial)
    head_out = weighted / totals[..., None]
    head_out = jnp.transpose(head_out, (2, 0, 1, 3)).reshape(local_rows, -1).astype(jnp.bfloat16)
    partial_value = jnp.dot(head_out, out_weight, preferred_element_type=jnp.float32)
    model_width = partial_value.shape[1]
    share_cols = model_width // lax.axis_size("tp")
    first_col = lax.axis_index("tp") * share_cols
    share_sum = sum_at_owner(partial_value.astype(jnp.bfloat16), "tp", 1)
    own_stream = lax.dynamic_slice_in_dim(stream, first_col, share_cols, 1)
    own_mid = (own_stream.astype(jnp.float32) + share_sum).astype(jnp.bfloat16)
    own_wide = own_mid.astype(jnp.float32)
    squares = lax.psum(jnp.sum(own_wide * own_wide, axis=-1), "tp")
    own_gain = lax.dynamic_slice_in_dim(mixer_gain, first_col, share_cols, 0)
    normed_part = own_wide * lax.rsqrt(squares / model_width + EPSILON)[:, None] * own_gain
    normed = gather_directly(normed_part.astype(jnp.bfloat16), "tp", 1)
    up_sums = jnp.dot(normed, up_whole, preferred_element_type=jnp.float32)
    hidden = jnp.square(jax.nn.relu(up_sums)).astype(jnp.bfloat16)
    down_part = jnp.dot(hidden, down_whole, preferred_element_type=jnp.float32)
    down_share = sum_at_owner(down_part.astype(jnp.bfloat16), "tp", 1)
    return (own_mid.astype(jnp.float32) + down_share).astype(jnp.bfloat16)


def solution(mesh):
    return jax.shard_map(
        shards,
        mesh=mesh,
        in_specs=(
            P("sp", "tp"),
            P("sp", "tp"),
            P("sp", "tp"),
            P(),
            P(),
            P("sp", None),
            P("tp", None),
            P(),
            P("sp", "tp"),
            P("tp", "sp"),
        ),
        out_specs=P("sp", "tp"),
        check_vma=False,
    )
```

profile of v0, /device:TPU:1, one launch (start us, length us, event | category | flops | bytes accessed | tf_op | source)
XLA Modules:
  0.0 399.9 jit_solution(15781413693797703937)
XLA Ops:
  6.6 1.1 copy.23
  7.8 0.8 mul.232
  9.3 0.9 copy.24
  10.9 1.7 pad_maximum_fusion.1
  12.7 1.1 copy.25
  14.0 0.8 mul.251
  16.6 83.7 %all-gather.3.cloned.1.call-done = bf16[16384,256]{0,1:T(8,128)(2,1)} async-done(((bf16[256,256]{0,1:T(8,128)(2,1)}), bf16[16384,256]{0,1:T(8,128)(2,1)}) %all-gather.3.cloned.1.call-update) | async-done | bytes 8388624 | tf_op jit(solution)/shard_map/all_gather | solution.py:35
  100.3 3.9 fusion.46
  104.2 3.2 copy.36
  107.4 4.3 %copy.26 = bf16[8,2048,2,64]{1,3,2,0:T(8,128)(2,1)} copy(bf16[8,2048,2,64]{1,0,3,2:T(8,128)(2,1)S(1)} %bitcast.85) | data formatting | bytes 8388608
  111.7 3.2 copy.37
  114.9 4.2 %copy.27 = bf16[8,2048,2,64]{1,3,2,0:T(8,128)(2,1)} copy(bf16[8,2048,2,64]{1,0,3,2:T(8,128)(2,1)S(1)} %bitcast.86) | data formatting | bytes 8388608
  119.2 204.9 %while.18 = (s32[]{:T(128)}, f32[2,4,256]{2,1,0:T(4,128)S(1)}, f32[2,4,256]{2,1,0:T(4,128)S(1)}, f32[2,4,256,64]{2,3,1,0:T(8,128)S(1)}, bf16[8,2048,2,64]{1,3,2,...) while((s32[]{:T(128)}, f32[2,4,256]{2,1,0:T(4,128)S(1)}, ...), condition=%wide.region_5.6_spmd.clone, body=%wide.region_2.5_spmd.clone.sunk | while | flops 1107699712 | bytes 52823140 | solution.py:138
  119.2 9.1 %bitcast_reduce_fusion.4 = (f32[2,4,256]{2,1,0:T(4,128)S(1)}, f32[2,2048,256,4]{2,1,3,0:T(8,128)}) fusion(bf16[256,2,4,64]{0,3,2,1:T(8,128)(2,1)S(1)} %get-tuple-element.276, bf16[8,2048,2,64]{1,3,2,0:T(8,128)(2,1)} %get-tuple-element.275, s32[]{:T(128)} %get-tuple-element.262), kind=kOutput, calls=%fused_computation.1.clone.1 | convolution fusion | flops 545257472 | bytes 17572352 | tf_op jit(solution)/shard_map/while/body/eval_jaxpr/qhgd,khd->hgqk/dot_general | solution.py:93
  128.3 8.6 %fusion.60 = f32[2,4,256]{2,1,0:T(4,128)S(1)} fusion(f32[2,2048,256,4]{2,1,3,0:T(8,128)} %get-tuple-element.250, f32[2,4,256]{2,1,0:T(4,128)S(1)} %select_maximum_fusion.2), kind=kLoop, calls=%fused_computation.4.clone.1 | loop fusion | flops 12580864 | bytes 16793600 | tf_op jit(solution)/shard_map/while/body/eval_jaxpr/reduce_sum | solution.py:98
  137.0 7.5 %fusion.62 = f32[2,4,256,64]{2,3,1,0:T(8,128)S(1)} fusion(f32[2,2048,256,4]{2,1,3,0:T(8,128)} %get-tuple-element.250, f32[2,4,256]{2,1,0:T(4,128)S(1)} %select_maximum_fusion.2, f32[2,4,256,64]{2,3,1,0:T(8,128)S(1)} %get-tuple-element.265, bf16[8,2048,2,64]{1,3,2,0:T(8,128)(2,1)} %get-tuple-element.277, s32[]{:T(128)} %get-tuple-element.262, ...), kind=kOutput, calls=%fused_computation.6.clone.1 | convolution fusion | flops 549847040 | bytes 18366976 | tf_op jit(solution)/shard_map/while/body/eval_jaxpr/hgqk,khd->hgqd/dot_general | solution.py:99
  144.5 9.5 %bitcast_reduce_fusion.4 = (f32[2,4,256]{2,1,0:T(4,128)S(1)}, f32[2,2048,256,4]{2,1,3,0:T(8,128)}) fusion(bf16[256,2,4,64]{0,3,2,1:T(8,128)(2,1)S(1)} %get-tuple-element.276, bf16[8,2048,2,64]{1,3,2,0:T(8,128)(2,1)} %get-tuple-element.275, s32[]{:T(128)} %get-tuple-element.262), kind=kOutput, calls=%fused_computation.1.clone.1 | convolution fusion | flops 545257472 | bytes 17572352 | tf_op jit(solution)/shard_map/while/body/eval_jaxpr/qhgd,khd->hgqk/dot_general | solution.py:93
  154.0 9.1 %fusion.60 = f32[2,4,256]{2,1,0:T(4,128)S(1)} fusion(f32[2,2048,256,4]{2,1,3,0:T(8,128)} %get-tuple-element.250, f32[2,4,256]{2,1,0:T(4,128)S(1)} %select_maximum_fusion.2), kind=kLoop, calls=%fused_computation.4.clone.1 | loop fusion | flops 12580864 | bytes 16793600 | tf_op jit(solution)/shard_map/while/body/eval_jaxpr/reduce_sum | solution.py:98
  163.2 8.1 %fusion.62 = f32[2,4,256,64]{2,3,1,0:T(8,128)S(1)} fusion(f32[2,2048,256,4]{2,1,3,0:T(8,128)} %get-tuple-element.250, f32[2,4,256]{2,1,0:T(4,128)S(1)} %select_maximum_fusion.2, f32[2,4,256,64]{2,3,1,0:T(8,128)S(1)} %get-tuple-element.265, bf16[8,2048,2,64]{1,3,2,0:T(8,128)(2,1)} %get-tuple-element.277, s32[]{:T(128)} %get-tuple-element.262, ...), kind=kOutput, calls=%fused_computation.6.clone.1 | convolution fusion | flops 549847040 | bytes 18366976 | tf_op jit(solution)/shard_map/while/body/eval_jaxpr/hgqk,khd->hgqd/dot_general | solution.py:99
  171.3 9.7 %bitcast_reduce_fusion.4 = (f32[2,4,256]{2,1,0:T(4,128)S(1)}, f32[2,2048,256,4]{2,1,3,0:T(8,128)}) fusion(bf16[256,2,4,64]{0,3,2,1:T(8,128)(2,1)S(1)} %get-tuple-element.276, bf16[8,2048,2,64]{1,3,2,0:T(8,128)(2,1)} %get-tuple-element.275, s32[]{:T(128)} %get-tuple-element.262), kind=kOutput, calls=%fused_computation.1.clone.1 | convolution fusion | flops 545257472 | bytes 17572352 | tf_op jit(solution)/shard_map/while/body/eval_jaxpr/qhgd,khd->hgqk/dot_general | solution.py:93
  181.1 8.9 %fusion.60 = f32[2,4,256]{2,1,0:T(4,128)S(1)} fusion(f32[2,2048,256,4]{2,1,3,0:T(8,128)} %get-tuple-element.250, f32[2,4,256]{2,1,0:T(4,128)S(1)} %select_maximum_fusion.2), kind=kLoop, calls=%fused_computation.4.clone.1 | loop fusion | flops 12580864 | bytes 16793600 | tf_op jit(solution)/shard_map/while/body/eval_jaxpr/reduce_sum | solution.py:98
  190.0 7.8 %fusion.62 = f32[2,4,256,64]{2,3,1,0:T(8,128)S(1)} fusion(f32[2,2048,256,4]{2,1,3,0:T(8,128)} %get-tuple-element.250, f32[2,4,256]{2,1,0:T(4,128)S(1)} %select_maximum_fusion.2, f32[2,4,256,64]{2,3,1,0:T(8,128)S(1)} %get-tuple-element.265, bf16[8,2048,2,64]{1,3,2,0:T(8,128)(2,1)} %get-tuple-element.277, s32[]{:T(128)} %get-tuple-element.262, ...), kind=kOutput, calls=%fused_computation.6.clone.1 | convolution fusion | flops 549847040 | bytes 18366976 | tf_op jit(solution)/shard_map/while/body/eval_jaxpr/hgqk,khd->hgqd/dot_general | solution.py:99
  197.9 9.1 %bitcast_reduce_fusion.4 = (f32[2,4,256]{2,1,0:T(4,128)S(1)}, f32[2,2048,256,4]{2,1,3,0:T(8,128)}) fusion(bf16[256,2,4,64]{0,3,2,1:T(8,128)(2,1)S(1)} %get-tuple-element.276, bf16[8,2048,2,64]{1,3,2,0:T(8,128)(2,1)} %get-tuple-element.275, s32[]{:T(128)} %get-tuple-element.262), kind=kOutput, calls=%fused_computation.1.clone.1 | convolution fusion | flops 545257472 | bytes 17572352 | tf_op jit(solution)/shard_map/while/body/eval_jaxpr/qhgd,khd->hgqk/dot_general | solution.py:93
  207.0 8.5 %fusion.60 = f32[2,4,256]{2,1,0:T(4,128)S(1)} fusion(f32[2,2048,256,4]{2,1,3,0:T(8,128)} %get-tuple-element.250, f32[2,4,256]{2,1,0:T(4,128)S(1)} %select_maximum_fusion.2), kind=kLoop, calls=%fused_computation.4.clone.1 | loop fusion | flops 12580864 | bytes 16793600 | tf_op jit(solution)/shard_map/while/body/eval_jaxpr/reduce_sum | solution.py:98
  215.6 7.5 %fusion.62 = f32[2,4,256,64]{2,3,1,0:T(8,128)S(1)} fusion(f32[2,2048,256,4]{2,1,3,0:T(8,128)} %get-tuple-element.250, f32[2,4,256]{2,1,0:T(4,128)S(1)} %select_maximum_fusion.2, f32[2,4,256,64]{2,3,1,0:T(8,128)S(1)} %get-tuple-element.265, bf16[8,2048,2,64]{1,3,2,0:T(8,128)(2,1)} %get-tuple-element.277, s32[]{:T(128)} %get-tuple-element.262, ...), kind=kOutput, calls=%fused_computation.6.clone.1 | convolution fusion | flops 549847040 | bytes 18366976 | tf_op jit(solution)/shard_map/while/body/eval_jaxpr/hgqk,khd->hgqd/dot_general | solution.py:99
  223.1 9.1 %bitcast_reduce_fusion.4 = (f32[2,4,256]{2,1,0:T(4,128)S(1)}, f32[2,2048,256,4]{2,1,3,0:T(8,128)}) fusion(bf16[256,2,4,64]{0,3,2,1:T(8,128)(2,1)S(1)} %get-tuple-element.276, bf16[8,2048,2,64]{1,3,2,0:T(8,128)(2,1)} %get-tuple-element.275, s32[]{:T(128)} %get-tuple-element.262), kind=kOutput, calls=%fused_computation.1.clone.1 | convolution fusion | flops 545257472 | bytes 17572352 | tf_op jit(solution)/shard_map/while/body/eval_jaxpr/qhgd,khd->hgqk/dot_general | solution.py:93
  232.3 8.5 %fusion.60 = f32[2,4,256]{2,1,0:T(4,128)S(1)} fusion(f32[2,2048,256,4]{2,1,3,0:T(8,128)} %get-tuple-element.250, f32[2,4,256]{2,1,0:T(4,128)S(1)} %select_maximum_fusion.2), kind=kLoop, calls=%fused_computation.4.clone.1 | loop fusion | flops 12580864 | bytes 16793600 | tf_op jit(solution)/shard_map/while/body/eval_jaxpr/reduce_sum | solution.py:98
  240.8 7.5 %fusion.62 = f32[2,4,256,64]{2,3,1,0:T(8,128)S(1)} fusion(f32[2,2048,256,4]{2,1,3,0:T(8,128)} %get-tuple-element.250, f32[2,4,256]{2,1,0:T(4,128)S(1)} %select_maximum_fusion.2, f32[2,4,256,64]{2,3,1,0:T(8,128)S(1)} %get-tuple-element.265, bf16[8,2048,2,64]{1,3,2,0:T(8,128)(2,1)} %get-tuple-element.277, s32[]{:T(128)} %get-tuple-element.262, ...), kind=kOutput, calls=%fused_computation.6.clone.1 | convolution fusion | flops 549847040 | bytes 18366976 | tf_op jit(solution)/shard_map/while/body/eval_jaxpr/hgqk,khd->hgqd/dot_general | solution.py:99
  248.4 9.1 %bitcast_reduce_fusion.4 = (f32[2,4,256]{2,1,0:T(4,128)S(1)}, f32[2,2048,256,4]{2,1,3,0:T(8,128)}) fusion(bf16[256,2,4,64]{0,3,2,1:T(8,128)(2,1)S(1)} %get-tuple-element.276, bf16[8,2048,2,64]{1,3,2,0:T(8,128)(2,1)} %get-tuple-element.275, s32[]{:T(128)} %get-tuple-element.262), kind=kOutput, calls=%fused_computation.1.clone.1 | convolution fusion | flops 545257472 | bytes 17572352 | tf_op jit(solution)/shard_map/while/body/eval_jaxpr/qhgd,khd->hgqk/dot_general | solution.py:93
  257.5 8.5 %fusion.60 = f32[2,4,256]{2,1,0:T(4,128)S(1)} fusion(f32[2,2048,256,4]{2,1,3,0:T(8,128)} %get-tuple-element.250, f32[2,4,256]{2,1,0:T(4,128)S(1)} %select_maximum_fusion.2), kind=kLoop, calls=%fused_computation.4.clone.1 | loop fusion | flops 12580864 | bytes 16793600 | tf_op jit(solution)/shard_map/while/body/eval_jaxpr/reduce_sum | solution.py:98
  266.1 7.5 %fusion.62 = f32[2,4,256,64]{2,3,1,0:T(8,128)S(1)} fusion(f32[2,2048,256,4]{2,1,3,0:T(8,128)} %get-tuple-element.250, f32[2,4,256]{2,1,0:T(4,128)S(1)} %select_maximum_fusion.2, f32[2,4,256,64]{2,3,1,0:T(8,128)S(1)} %get-tuple-element.265, bf16[8,2048,2,64]{1,3,2,0:T(8,128)(2,1)} %get-tuple-element.277, s32[]{:T(128)} %get-tuple-element.262, ...), kind=kOutput, calls=%fused_computation.6.clone.1 | convolution fusion | flops 549847040 | bytes 18366976 | tf_op jit(solution)/shard_map/while/body/eval_jaxpr/hgqk,khd->hgqd/dot_general | solution.py:99
  273.6 9.1 %bitcast_reduce_fusion.4 = (f32[2,4,256]{2,1,0:T(4,128)S(1)}, f32[2,2048,256,4]{2,1,3,0:T(8,128)}) fusion(bf16[256,2,4,64]{0,3,2,1:T(8,128)(2,1)S(1)} %get-tuple-element.276, bf16[8,2048,2,64]{1,3,2,0:T(8,128)(2,1)} %get-tuple-element.275, s32[]{:T(128)} %get-tuple-element.262), kind=kOutput, calls=%fused_computation.1.clone.1 | convolution fusion | flops 545257472 | bytes 17572352 | tf_op jit(solution)/shard_map/while/body/eval_jaxpr/qhgd,khd->hgqk/dot_general | solution.py:93
  282.8 8.5 %fusion.60 = f32[2,4,256]{2,1,0:T(4,128)S(1)} fusion(f32[2,2048,256,4]{2,1,3,0:T(8,128)} %get-tuple-element.250, f32[2,4,256]{2,1,0:T(4,128)S(1)} %select_maximum_fusion.2), kind=kLoop, calls=%fused_computation.4.clone.1 | loop fusion | flops 12580864 | bytes 16793600 | tf_op jit(solution)/shard_map/while/body/eval_jaxpr/reduce_sum | solution.py:98
  291.3 7.5 %fusion.62 = f32[2,4,256,64]{2,3,1,0:T(8,128)S(1)} fusion(f32[2,2048,256,4]{2,1,3,0:T(8,128)} %get-tuple-element.250, f32[2,4,256]{2,1,0:T(4,128)S(1)} %select_maximum_fusion.2, f32[2,4,256,64]{2,3,1,0:T(8,128)S(1)} %get-tuple-element.265, bf16[8,2048,2,64]{1,3,2,0:T(8,128)(2,1)} %get-tuple-element.277, s32[]{:T(128)} %get-tuple-element.262, ...), kind=kOutput, calls=%fused_computation.6.clone.1 | convolution fusion | flops 549847040 | bytes 18366976 | tf_op jit(solution)/shard_map/while/body/eval_jaxpr/hgqk,khd->hgqd/dot_general | solution.py:99
  298.9 9.1 %bitcast_reduce_fusion.4 = (f32[2,4,256]{2,1,0:T(4,128)S(1)}, f32[2,2048,256,4]{2,1,3,0:T(8,128)}) fusion(bf16[256,2,4,64]{0,3,2,1:T(8,128)(2,1)S(1)} %get-tuple-element.276, bf16[8,2048,2,64]{1,3,2,0:T(8,128)(2,1)} %get-tuple-element.275, s32[]{:T(128)} %get-tuple-element.262), kind=kOutput, calls=%fused_computation.1.clone.1 | convolution fusion | flops 545257472 | bytes 17572352 | tf_op jit(solution)/shard_map/while/body/eval_jaxpr/qhgd,khd->hgqk/dot_general | solution.py:93
  308.0 8.5 %fusion.60 = f32[2,4,256]{2,1,0:T(4,128)S(1)} fusion(f32[2,2048,256,4]{2,1,3,0:T(8,128)} %get-tuple-element.250, f32[2,4,256]{2,1,0:T(4,128)S(1)} %select_maximum_fusion.2), kind=kLoop, calls=%fused_computation.4.clone.1 | loop fusion | flops 12580864 | bytes 16793600 | tf_op jit(solution)/shard_map/while/body/eval_jaxpr/reduce_sum | solution.py:98
  316.6 7.5 %fusion.62 = f32[2,4,256,64]{2,3,1,0:T(8,128)S(1)} fusion(f32[2,2048,256,4]{2,1,3,0:T(8,128)} %get-tuple-element.250, f32[2,4,256]{2,1,0:T(4,128)S(1)} %select_maximum_fusion.2, f32[2,4,256,64]{2,3,1,0:T(8,128)S(1)} %get-tuple-element.265, bf16[8,2048,2,64]{1,3,2,0:T(8,128)(2,1)} %get-tuple-element.277, s32[]{:T(128)} %get-tuple-element.262, ...), kind=kOutput, calls=%fused_computation.6.clone.1 | convolution fusion | flops 549847040 | bytes 18366976 | tf_op jit(solution)/shard_map/while/body/eval_jaxpr/hgqk,khd->hgqd/dot_general | solution.py:99
  324.9 1.1 copy.41
  326.0 4.0 all-to-all-start
  330.0 0.8 dynamic_slice.21
  330.7 13.7 %all-to-all-done = bf16[4,256,512]{2,1,0:T(8,128)(2,1)S(1)} async-done(((bf16[4,256,512]{2,1,0:T(8,128)(2,1)}), bf16[4,256,512]{2,1,0:T(8,128)(2,1)S(1)}, u32[]{:S(2)}, u32[]{:S(2)}) %all-to-all-start) | async-done | bytes 1048608 | tf_op jit(solution)/shard_map/all_to_all | solution.py:46
  344.6 1.1 fusion.36
  345.7 6.9 %psum.7 = f32[256]{0:T(256)S(1)} all-reduce(f32[256]{0:T(256)S(1)} %get-tuple-element.186), channel_id=1, replica_groups=mesh['sp'=64,'tp'=4] {'tp'}, use_global_device_ids=true, to_apply=%region_8.9 | all-reduce | flops 256 | bytes 2048 | tf_op jit(solution)/shard_map/psum | solution.py:149
  353.0 13.7 %all_to_all.15 = bf16[4,256,512]{1,2,0:T(8,128)(2,1)S(1)} all-to-all(bf16[4,256,512]{1,2,0:T(8,128)(2,1)S(1)} %broadcast_in_dim.15), channel_id=1, replica_groups=mesh['sp'=64,'tp'=4] {'tp'}, dimensions={0} | all-to-all | bytes 2097152 | tf_op jit(solution)/shard_map/all_to_all | solution.py:58
  366.7 11.3 %fusion.30 = bf16[256,2048]{1,0:T(8,128)(2,1)} fusion(bf16[2048,4096]{1,0:T(8,128)(2,1)} %all-gather.5.cloned.1.call-done, bf16[256,2048]{0,1:T(8,128)(2,1)S(1)} %bitcast.92), kind=kOutput, calls=%fused_computation.28 | convolution fusion | flops 4297064448 | bytes 18874368 | tf_op jit(solution)/shard_map/dot_general | solution.py:155
  378.0 1.3 copy.40
  379.3 12.9 %all_to_all.16 = bf16[4,256,512]{2,1,0:T(8,128)(2,1)S(1)} all-to-all(bf16[4,256,512]{2,1,0:T(8,128)(2,1)S(1)} %bitcast.91), channel_id=1, replica_groups=mesh['sp'=64,'tp'=4] {'tp'}, dimensions={0} | all-to-all | bytes 2097152 | tf_op jit(solution)/shard_map/all_to_all | solution.py:46
  392.3 0.8 fusion.39
  (61 shorter events, 5.2 us)
Async XLA Ops:
  6.5 317.6 %copy-start = (bf16[512,2048]{1,0:T(8,128)(2,1)S(1)}, bf16[512,2048]{1,0:T(8,128)(2,1)}, u32[]{:S(2)}) copy-start(bf16[512,2048]{1,0:T(8,128)(2,1)} %param.18) | copy-start | bytes 6291460
  6.5 93.8 %all-gather.3.cloned.1.call-start = ((), (), s32[]{:S(2)}) async-start(), calls=%async_computation.3 | async-start | bytes 8519680 | tf_op jit(solution)/shard_map/all_gather | solution.py:35
  10.9 355.8 %all-gather.5.cloned.1.call-start = ((), (), s32[]{:S(2)}) async-start(), calls=%async_computation.4 | async-start | bytes 17039360 | tf_op jit(solution)/shard_map/all_gather | solution.py:19
  326.0 18.5 %all-to-all-start = ((bf16[4,256,512]{2,1,0:T(8,128)(2,1)}), bf16[4,256,512]{2,1,0:T(8,128)(2,1)S(1)}, u32[]{:S(2)}, u32[]{:S(2)}) async-start(bf16[4,256,512]{2,1,0:T(8,128)(2,1)} %bitcast.89), calls=%async_computation | async-start | bytes 2097152 | tf_op jit(solution)/shard_map/all_to_all | solution.py:46
Sparse Core Ops, SparseCore 0:
  11.0 89.2 all-gather.2
  103.1 99.6 all-gather.4
where the time goes:
time: 407 us; the launch traced here: 400 us
  matrix products  147 us (36%)
  waiting for transfers between devices  97.5 us (24%)
  other arithmetic  76.6 us (19%)
  blocking collectives  33.5 us (8%)
  local copies, waits for them, and re-layouts  27.3 us (7%)
  between operations  13.7 us (3%)
    all_gather x1, waiting for transfers between devices, sent_together(): lax.all_gather(both, axis, axis=dim, tiled=True)  83.7 us
    dot_general x8, matrix products, attend_block(): jnp.einsum('qhgd,khd->hgqk', grouped, key_block, preferred_element_type=j...  74 us
    reduce_sum x8, other arithmetic, attend_block(): totals = totals * rescale + jnp.sum(exps, axis=-1)  69.4 us
    dot_general x8, matrix products, attend_block(): jnp.einsum('hgqk,khd->hgqd', exps.astype(jnp.bfloat16), value_block, pref...  61 us
    unnamed x9, local copies, waits for them, and re-layouts  18.1 us
    all_to_all x1, blocking collectives, copy_for_each(): return lax.all_to_all(copies, axis, split_axis=0, concat_axis=0, tiled=True)  13.7 us
    all_to_all x1, waiting for transfers between devices, sum_at_owner(): lax.all_to_all(pieces, axis, split_axis=0, concat_axis=0, tiled=True)  13.7 us
    all_to_all x1, blocking collectives, sum_at_owner(): lax.all_to_all(pieces, axis, split_axis=0, concat_axis=0, tiled=True)  12.9 us
  transfers between devices with their start and end apart: 3, of which 2 were waited for; matrix products, arithmetic and copies ran while one was open for 58% of the time, Pallas kernels for 0%

commit v1 on v0

v1 whole, which is shorter than its diff:
```python
import functools
import math

import jax
import jax.numpy as jnp
from jax import lax
from jax.experimental import pallas as pl
from jax.experimental.pallas import tpu as pltpu
from jax.sharding import PartitionSpec as P

HD = 64
GRID_W = 64
EPSILON = 1e-06
NZ, NY, NC = 8, 4, 2
SCALE = math.log2(math.e) / math.sqrt(HD)
MESH = pl.DeviceIdType.MESH
ORDER = (0, 1, 7, 2, 6, 3, 5, 4)


def prepare(projected, gain_vec, offset):
    row_count = projected.shape[0]
    head_count = projected.shape[1] // HD
    widened = projected.astype(jnp.float32).reshape(row_count, head_count, HD)
    widened = (
        widened
        * lax.rsqrt(jnp.mean(widened * widened, axis=-1, keepdims=True) + EPSILON)
        * gain_vec
    )
    position = offset + jnp.arange(row_count, dtype=jnp.int32)
    grid_row = (position // GRID_W).astype(jnp.float32)
    grid_col = (position % GRID_W).astype(jnp.float32)
    half_dim = HD // 2
    inverse = 1.0 / jnp.power(10000.0, jnp.arange(0, half_dim, 2, dtype=jnp.float32) / half_dim)
    angle = jnp.concatenate([grid_row[:, None] * inverse, grid_col[:, None] * inverse], axis=-1)
    cosine = jnp.cos(angle)[:, None, :]
    sine_table = jnp.sin(angle)[:, None, :]
    paired = widened.reshape(row_count, head_count, half_dim, 2)
    former = paired[..., 0]
    latter = paired[..., 1]
    rotated = jnp.stack(
        [former * cosine - latter * sine_table, former * sine_table + latter * cosine], axis=-1
    )
    return rotated.reshape(row_count, head_count, HD).astype(jnp.bfloat16)


class Place:
    def __init__(self):
        me = lax.axis_index("sp")
        self.me = me
        self.core = lax.rem(me, NC)
        self.y = lax.rem(me // NC, NY)
        self.z = me // (NC * NY)

    def zat(self, d):
        return lax.rem(self.z + (d + NZ) % NZ, NZ)

    def yat(self, d):
        return lax.rem(self.y + (d + NY) % NY, NY)

    def dev(self, dz=0, dy=0, other=False):
        core = 1 - self.core if other else self.core
        return (self.zat(dz) * NY + self.yat(dy)) * NC + core


class Mail:
    def __init__(self, place, send_sems, recv_sems):
        self.at, self.ss, self.rs, self.sent = place, send_sems, recv_sems, []

    def copy(self, key, ref, target):
        return pltpu.make_async_remote_copy(
            src_ref=ref,
            dst_ref=ref,
            send_sem=self.ss.at[key],
            recv_sem=self.rs.at[key],
            device_id={"sp": target},
            device_id_type=MESH,
        )

    def send(self, key, ref, target):
        self.copy(key, ref(), target()).start()
        self.sent.append((key, ref, target))

    def got(self, key, ref):
        self.copy(key, ref, self.at.dev(0, 1)).wait_recv()

    def finish(self):
        for key, ref, target in self.sent:
            self.copy(key, ref(), target()).wait_send()


class ZFirst(Mail):
    SEMS = 48

    def __init__(self, buf, half, *rest):
        super().__init__(*rest)
        self.buf, self.half = buf, half

    def slot(self, r, dy=0):
        return self.buf.at[self.at.zat(r), self.at.yat(dy), self.at.core]

    def part(self, r, dy, second):
        return self.slot(r, dy).at[pl.ds(self.half if second else 0, self.half)]

    def along_y(self, r):
        r = r % NZ
        self.send(8 + r, lambda r=r: self.slot(r), lambda: self.at.dev(0, 1))
        self.send(16 + r, lambda r=r: self.slot(r), lambda: self.at.dev(0, -1))

    def a(self, d):
        if d == 0:
            self.send(0, lambda: self.slot(0), lambda: self.at.dev(1))
            self.send(4, lambda: self.slot(0), lambda: self.at.dev(-1))
            self.along_y(0)
            return
        if d == 4:
            self.got(3, self.part(4, 0, False))
            self.got(7, self.part(4, 0, True))
            self.along_y(4)
            return
        self.got(d - 1, self.slot(-d))
        if d < 3:
            self.send(d, lambda: self.slot(-d), lambda: self.at.dev(1))
        else:
            self.send(3, lambda: self.part(-3, 0, False), lambda: self.at.dev(1))
        self.got(3 + d, self.slot(d))
        if d < 3:
            self.send(4 + d, lambda: self.slot(d), lambda: self.at.dev(-1))
        else:
            self.send(7, lambda: self.part(3, 0, True), lambda: self.at.dev(-1))
        self.along_y(-d)
        self.along_y(d)

    def each(self, d):
        return (0,) if d == 0 else (4,) if d == 4 else (d, NZ - d)

    def b(self, d):
        for r in self.each(d):
            self.got(8 + r, self.slot(r, -1))
            self.send(24 + r, lambda r=r: self.part(r, -1, False), lambda: self.at.dev(0, 1))
            self.got(16 + r, self.slot(r, 1))
            self.send(32 + r, lambda r=r: self.part(r, 1, True), lambda: self.at.dev(0, -1))

    def c(self, d):
        for r in self.each(d):
            self.got(24 + r, self.part(r, 2, False))
            self.got(32 + r, self.part(r, 2, True))
            self.send(40 + r, lambda r=r: self.buf.at[self.at.zat(r), :, self.at.core], lambda: self.at.dev(other=True))

    def w(self, d):
        for r in self.each(d):
            self.got(40 + r, self.buf.at[self.at.zat(r), :, 1 - self.at.core])


class YFirst(Mail):
    SEMS = 20

    def __init__(self, buf, half, *rest):
        super().__init__(*rest)
        self.buf, self.half = buf, half

    def slot(self, dy):
        return self.buf.at[self.at.z, self.at.yat(dy), self.at.core]

    def part(self, dy, second):
        return self.slot(dy).at[pl.ds(self.half if second else 0, self.half)]

    def column(self, r):
        return self.buf.at[self.at.zat(r), :, self.at.core]

    def pair(self, r, second):
        return self.buf.at[self.at.zat(r), pl.ds(2 if second else 0, 2), self.at.core]

    def over(self, r):
        self.send(12 + r % NZ, lambda r=r: self.column(r), lambda: self.at.dev(other=True))

    def s1(self):
        self.send(0, lambda: self.slot(0), lambda: self.at.dev(0, 1))
        self.send(1, lambda: self.slot(0), lambda: self.at.dev(0, -1))

    def s2(self):
        self.got(0, self.slot(-1))
        self.send(2, lambda: self.part(-1, False), lambda: self.at.dev(0, 1))
        self.got(1, self.slot(1))
        self.send(3, lambda: self.part(1, True), lambda: self.at.dev(0, -1))

    def s3(self):
        self.got(2, self.part(2, False))
        self.got(3, self.part(2, True))
        self.send(4, lambda: self.column(0), lambda: self.at.dev(1))
        self.send(8, lambda: self.column(0), lambda: self.at.dev(-1))
        self.over(0)

    def z(self, d):
        if d == 4:
            self.got(7, self.pair(4, False))
            self.got(11, self.pair(4, True))
            self.over(4)
            return
        self.got(3 + d, self.column(-d))
        if d < 3:
            self.send(4 + d, lambda: self.column(-d), lambda: self.at.dev(1))
        else:
            self.send(7, lambda: self.pair(-3, False), lambda: self.at.dev(1))
        self.got(7 + d, self.column(d))
        if d < 3:
            self.send(8 + d, lambda: self.column(d), lambda: self.at.dev(-1))
        else:
            self.send(11, lambda: self.pair(3, True), lambda: self.at.dev(-1))
        self.over(-d)
        self.over(d)

    def w(self):
        for r in range(NZ):
            self.got(12 + r, self.buf.at[self.at.zat(r), :, 1 - self.at.core])


def attend(kv, q_ref, s_scr, acc, peak, zs, h):
    tiles, width = 4, 256
    where = [(y, c) for y in range(NY) for c in range(NC)]

    def scores(j):
        top = None
        for a, (y, c) in enumerate(where):
            t = jnp.dot(
                kv[zs, y, c, 0:256, :],
                q_ref[h, :, j * width : (j + 1) * width],
                preferred_element_type=jnp.float32,
            )
            s_scr[j % 2, a * 256 : (a + 1) * 256, :] = t
            t = jnp.max(t.reshape(32, 8, width), axis=0)
            top = t if top is None else jnp.maximum(top, t)
        return top

    ones = jnp.ones((16, 256), jnp.bfloat16)
    later = scores(0)
    for j in range(tiles):
        top = later
        if j + 1 < tiles:
            later = scores(j + 1)
        cols = slice(j * width, (j + 1) * width)
        before = peak[h, 0:1, cols]
        now = jnp.maximum(before, jnp.max(top, axis=0, keepdims=True) * SCALE)
        peak[h, 0:1, cols] = now
        rescale = jnp.exp2(before - now)
        added = None
        for a, (y, c) in enumerate(where):
            exps = jnp.exp2(s_scr[j % 2, a * 256 : (a + 1) * 256, :] * SCALE - now)
            first = kv[zs, y, c, pl.ds(pl.multiple_of(256 + h * HD, HD), HD), :]
            second = kv[zs, y, c, pl.ds(pl.multiple_of(384 + h * HD, HD), HD), :]
            left = jnp.concatenate([jnp.concatenate([first, second], axis=1), ones], axis=0)
            term = jnp.dot(left, exps.astype(jnp.bfloat16), preferred_element_type=jnp.float32)
            added = term if added is None else added + term
        acc[h, :, cols] = acc[h, :, cols] * rescale + added


def gather_attend_kernel(
    q_ref, kv_in, up_in, down_in, o_ref, up_all, down_all,
    kv, s_scr, acc, peak, kv_s, kv_r, up_s, up_r, down_s, down_r, own_sem,
):
    at = Place()
    own = [
        pltpu.make_async_copy(src, dst.at[at.z, at.y, at.core], own_sem.at[k])
        for k, (src, dst) in enumerate(((kv_in, kv), (up_in, up_all), (down_in, down_all)))
    ]
    for copy in own:
        copy.start()
    barrier = pltpu.get_barrier_semaphore()
    for near in (at.dev(1), at.dev(-1), at.dev(0, 1), at.dev(0, -1), at.dev(other=True)):
        pl.semaphore_signal(barrier, inc=1, device_id={"sp": near}, device_id_type=MESH)
    acc[...] = jnp.zeros_like(acc)
    peak[...] = jnp.full_like(peak, -1e30)
    pl.semaphore_wait(barrier, 5)
    pair = ZFirst(kv, 256, at, kv_s, kv_r)
    up = YFirst(up_all, 16, at, up_s, up_r)
    down = ZFirst(down_all, 16, at, down_s, down_r)

    own[0].wait()
    pair.a(0)
    own[1].wait()
    own[2].wait()
    pair.b(0)
    pair.a(1)
    up.s1()
    pair.c(0)
    pair.w(0)
    polls = {
        1: (lambda: pair.b(1), lambda: pair.a(2), up.s2),
        2: (lambda: pair.c(1), up.s3, lambda: pair.w(1)),
        3: (lambda: pair.a(3),),
        4: (lambda: pair.b(2),),
        5: (lambda: pair.c(2), lambda: pair.a(4)),
        6: (lambda: up.z(1), lambda: down.a(0), lambda: pair.w(2)),
        7: (lambda: pair.b(3),),
        8: (lambda: pair.c(3), lambda: pair.b(4), lambda: down.a(1), lambda: down.b(0)),
        9: (lambda: pair.c(4),),
        10: (lambda: pair.w(3), lambda: up.z(2), lambda: down.a(2), lambda: down.b(1), lambda: down.c(0)),
        12: (lambda: down.a(3), lambda: down.b(2), lambda: down.c(1)),
        13: (lambda: pair.w(4),),
        14: (lambda: up.z(3), lambda: down.a(4), lambda: down.b(3), lambda: down.c(2)),
    }

    def step(n, carry):
        for k, todo in polls.items():

            @pl.when(n == k)
            def _(todo=todo):
                for do in todo:
                    do()

        turn = n // 2
        r = jnp.where(lax.rem(turn, 2) == 1, turn // 2 + 1, NZ - turn // 2)
        attend(kv, q_ref, s_scr, acc, peak, lax.rem(at.z + r, NZ), lax.rem(n, 2))
        return carry

    lax.fori_loop(0, 2 * NZ, step, 0)
    o_ref[...] = (acc[:, 0:HD, :] / acc[:, HD : HD + 1, :]).astype(jnp.bfloat16)
    down.b(4)
    down.c(3)
    up.z(4)
    down.c(4)
    up.w()
    for d in range(5):
        down.w(d)
    for mail in (pair, up, down):
        mail.finish()


def gather_attend(q_wide, kv_block, up_block, down_block):
    anywhere = pl.BlockSpec(memory_space=pl.ANY)
    vmem = pl.BlockSpec(memory_space=pltpu.VMEM)
    sems = [pltpu.SemaphoreType.DMA((n,)) for n in (48, 48, 20, 20, 48, 48, 3)]
    whole = jax.ShapeDtypeStruct((NZ, NY, NC, *up_block.shape), jnp.bfloat16)
    return pl.pallas_call(
        gather_attend_kernel,
        name="gather_attend",
        out_shape=(jax.ShapeDtypeStruct((2, HD, 1024), jnp.bfloat16), whole, whole),
        in_specs=[vmem, anywhere, anywhere, anywhere],
        out_specs=(vmem, anywhere, anywhere),
        scratch_shapes=[
            pltpu.VMEM((NZ, NY, NC, 512, 128), jnp.bfloat16),
            pltpu.VMEM((2, 2048, 256), jnp.float32),
            pltpu.VMEM((2, 80, 1024), jnp.float32),
            pltpu.VMEM((2, 8, 1024), jnp.float32),
            *sems,
        ],
        compiler_params=pltpu.CompilerParams(
            collective_id=0, has_side_effects=True, vmem_limit_bytes=56 * 1024 * 1024
        ),
    )(q_wide, kv_block, up_block, down_block)


def in_blocks(x, dim, count):
    dims = x.shape
    pieces = x.reshape(*dims[:dim], count, dims[dim] // count, *dims[dim + 1 :])
    return jnp.moveaxis(pieces, dim, 0)


def sum_at_owner(x, axis, dim):
    pieces = in_blocks(x, dim, lax.axis_size(axis))
    arrived = lax.all_to_all(pieces, axis, split_axis=0, concat_axis=0, tiled=True)
    return arrived.astype(jnp.float32).sum(axis=0)


def laid_out(pieces, dim):
    pieces = jnp.moveaxis(pieces, 0, dim)
    dims = pieces.shape
    return pieces.reshape(*dims[:dim], dims[dim] * dims[dim + 1], *dims[dim + 2 :])


def gather_directly(x, axis, dim):
    copies = jnp.broadcast_to(x, (lax.axis_size(axis), *x.shape))
    return laid_out(lax.all_to_all(copies, axis, split_axis=0, concat_axis=0, tiled=True), dim)


def shards(
    queries,
    keys,
    values,
    query_gain,
    key_gain,
    stream,
    out_weight,
    mixer_gain,
    up_weight,
    down_weight,
):
    rows = queries.shape[0]
    offset = lax.axis_index("sp") * rows
    pq = prepare(queries, query_gain, offset)
    pq = jnp.transpose(pq.reshape(rows, 2, 4, HD), (1, 3, 2, 0)).reshape(2, HD, 4 * rows)
    none = jnp.zeros((1, HD, 4 * rows), jnp.bfloat16)
    q_wide = jnp.concatenate(
        [jnp.concatenate([pq[:1], none], axis=1), jnp.concatenate([none, pq[1:]], axis=1)], axis=0
    )
    pk = prepare(keys, key_gain, offset).reshape(rows, 128)
    v_turned = jnp.transpose(values.reshape(2, 128, 128), (0, 2, 1)).reshape(256, 128)
    kv_block = jnp.concatenate([pk, v_turned], axis=0)
    out, up_all, down_all = gather_attend(q_wide, kv_block, up_weight, down_weight.T)
    head_out = jnp.transpose(out.reshape(2, HD, 4, rows), (3, 0, 2, 1)).reshape(rows, -1)

    partial_value = jnp.dot(head_out, out_weight, preferred_element_type=jnp.float32)
    model_width = partial_value.shape[1]
    share_cols = model_width // lax.axis_size("tp")
    first_col = lax.axis_index("tp") * share_cols
    share_sum = sum_at_owner(partial_value.astype(jnp.bfloat16), "tp", 1)
    own_stream = lax.dynamic_slice_in_dim(stream, first_col, share_cols, 1)
    own_mid = (own_stream.astype(jnp.float32) + share_sum).astype(jnp.bfloat16)
    own_wide = own_mid.astype(jnp.float32)
    squares = lax.psum(jnp.sum(own_wide * own_wide, axis=-1), "tp")
    own_gain = lax.dynamic_slice_in_dim(mixer_gain, first_col, share_cols, 0)
    normed_part = own_wide * lax.rsqrt(squares / model_width + EPSILON)[:, None] * own_gain
    normed = gather_directly(normed_part.astype(jnp.bfloat16), "tp", 1)
    up_whole = up_all.reshape(model_width, -1)
    up_sums = jnp.dot(normed, up_whole, preferred_element_type=jnp.float32)
    hidden = jnp.square(jax.nn.relu(up_sums)).astype(jnp.bfloat16)
    down_turned = down_all.reshape(model_width, -1)
    down_part = lax.dot_general(
        hidden, down_turned, (((1,), (1,)), ((), ())), preferred_element_type=jnp.float32
    )
    down_share = sum_at_owner(down_part.astype(jnp.bfloat16), "tp", 1)
    return (own_mid.astype(jnp.float32) + down_share).astype(jnp.bfloat16)


def solution(mesh):
    return jax.shard_map(
        shards,
        mesh=mesh,
        in_specs=(
            P("sp", "tp"),
            P("sp", "tp"),
            P("sp", "tp"),
            P(),
            P(),
            P("sp", None),
            P("tp", None),
            P(),
            P("sp", "tp"),
            P("tp", "sp"),
        ),
        out_specs=P("sp", "tp"),
        check_vma=False,
    )
```

time: 407 us -> 202 us (0.50); the launches traced: 400 us -> 199 us
  matrix products: 147 us -> 12 us
  Pallas kernels: 0 us -> 119 us
  waiting for transfers between devices: 97.5 us -> 14.2 us
  other arithmetic: 76.6 us -> 6.16 us
  local copies, waits for them, and re-layouts: 27.3 us -> 8.76 us
  between operations: 13.7 us -> 0.24 us
    dot_general x17 -> x1, matrix products: 146 us -> 11.3 us  [shards(): lax.dot_general(hidden, down_turned, (((1,), (1,)), ((), ())), preferred_...]
    pallas_call x0 -> x1, Pallas kernels: none -> 119 us  [gather_attend(): pl.pallas_call(gather_attend_kernel, name='gather_attend', out_shape=(jax...]
    all_gather x2 -> x0, waiting for transfers between devices: 83.7 us -> none  [the longest x1 83.7 us: sent_together(): lax.all_gather(both, axis, axis=dim, tiled=True)]
    reduce_sum x8 -> x0, other arithmetic: 69.4 us -> none  [attend_block(): totals = totals * rescale + jnp.sum(exps, axis=-1)]
    unnamed x9 -> x7, local copies, waits for them, and re-layouts: 18.1 us -> 2.21 us
  transfers between devices with their start and end apart: 3 -> 1, of which waited for: 2 -> 1; matrix products, arithmetic and copies ran while one was open for 58% -> 0% of each run, Pallas kernels for 0% -> 0%
where the time goes in v1:
time: 202 us; the launch traced here: 199 us
  Pallas kernels  119 us (59%)
  blocking collectives  35 us (17%)
  waiting for transfers between devices  14.2 us (7%)
  matrix products  12 us (6%)
  local copies, waits for them, and re-layouts  8.76 us (4%)
  other arithmetic  6.16 us (3%)
  starting transfers between devices  4.01 us (2%)
    pallas_call x1, Pallas kernels, gather_attend(): pl.pallas_call(gather_attend_kernel, name='gather_attend', out_shape=(jax...  119 us
    all_to_all x1, blocking collectives, gather_directly(): lax.all_to_all(copies, axis, split_axis=0, concat_axis=0, tiled=True)  14.5 us
    all_to_all x1, waiting for transfers between devices, sum_at_owner(): lax.all_to_all(pieces, axis, split_axis=0, concat_axis=0, tiled=True)  14.2 us
    all_to_all x1, blocking collectives, sum_at_owner(): lax.all_to_all(pieces, axis, split_axis=0, concat_axis=0, tiled=True)  13.6 us
    dot_general x1, matrix products, shards(): lax.dot_general(hidden, down_turned, (((1,), (1,)), ((), ())), preferred_...  11.3 us
    psum x1, blocking collectives, shards(): squares = lax.psum(jnp.sum(own_wide * own_wide, axis=-1), 'tp')  6.88 us
  transfers between devices with their start and end apart: 1, of which 1 were waited for; matrix products, arithmetic and copies ran while one was open for 0% of the time, Pallas kernels for 0%

profile of v1, /device:TPU:1, one launch (start us, length us, event | category | flops | bytes accessed | tf_op | source)
XLA Modules:
  0.0 199.3 jit_solution(7927756128873824406)
XLA Ops:
  0.0 0.0 copy-start
  0.0 0.0 copy-start.1
  0.0 1.1 copy.23
  1.2 0.1 reshape.169
  1.2 1.1 copy.20
  2.3 0.1 bitcast_reduce_fusion
  2.4 0.3 reshape.168
  2.7 0.8 mul.195
  3.4 0.8 mul.214
  4.2 0.1 broadcast_multiply_fusion.1
  4.3 0.1 fusion.10
  4.4 0.1 multiply_multiply_fusion.1
  4.5 0.2 subtract_convert_fusion.1
  4.7 0.2 pad_maximum_fusion.2
  4.9 0.1 copy.25
  5.0 0.0 copy-done.1
  5.1 0.1 copy.24
  5.2 0.3 multiply_multiply_fusion
  5.5 0.7 subtract_convert_fusion
  6.1 0.6 pad_maximum_fusion
  6.8 0.1 convert_element_type.67
  6.9 0.7 pad_maximum_fusion.1.kv_in
  7.6 0.8 fusion.8.q_ref
  8.4 118.9 %gather_attend.1 = (bf16[2,64,1024]{2,1,0:T(8,128)(2,1)}, bf16[8,4,2,32,2048]{4,3,2,1,0:T(8,128)(2,1)}, bf16[8,4,2,32,2048]{4,3,2,1,0:T(8,128)(2,1)}) custom-call(bf16[2,128,1024]{2,1,0:T(8,128)(2,1)} %fusion.8.q_ref, bf16[512,128]{1,0:T(8,128)(2,1)} %pad_maximum_fusion.1.kv_in, bf16[32,2048]{1,0:T(8,128)(2,1)} %up_in.1, bf16[32,2048]{1,0:T(8,128)(2,1)} %bitcast.66), custom_call_target="tpu_custom_call" | custom-call | tf_op jit(solution)/shard_map/gather_attend/pallas_call | solution.py:333
  127.3 1.0 copy.40
  128.3 0.0 copy-done
  128.3 0.7 convolution_convert_fusion
  129.0 1.1 copy.39
  130.1 4.0 %all-to-all-start = ((bf16[4,256,512]{2,1,0:T(8,128)(2,1)}), bf16[4,256,512]{2,1,0:T(8,128)(2,1)S(1)}, u32[]{:S(2)}, u32[]{:S(2)}) async-start(bf16[4,256,512]{2,1,0:T(8,128)(2,1)} %bitcast.55), calls=%async_computation | async-start | bytes 2097152 | tf_op jit(solution)/shard_map/all_to_all | solution.py:360
  134.1 0.8 dynamic_slice.7
  134.9 14.2 %all-to-all-done = bf16[4,256,512]{2,1,0:T(8,128)(2,1)S(1)} async-done(((bf16[4,256,512]{2,1,0:T(8,128)(2,1)}), bf16[4,256,512]{2,1,0:T(8,128)(2,1)S(1)}, u32[]{:S(2)}, u32[]{:S(2)}) %all-to-all-start) | async-done | bytes 1048608 | tf_op jit(solution)/shard_map/all_to_all | solution.py:360
  149.1 0.1 convert_reduce_fusion.1
  149.2 1.1 fusion.4
  150.4 6.9 %psum.7 = f32[256]{0:T(256)S(1)} all-reduce(f32[256]{0:T(256)S(1)} %get-tuple-element.11), channel_id=1, replica_groups=mesh['sp'=64,'tp'=4] {'tp'}, use_global_device_ids=true, to_apply=%region_4.5 | all-reduce | flops 256 | bytes 2048 | tf_op jit(solution)/shard_map/psum | solution.py:409
  157.2 0.1 fusion.6
  157.4 0.1 copy.28
  157.5 0.1 broadcast_in_dim.2
  157.6 14.5 %all_to_all.15 = bf16[4,256,512]{1,2,0:T(8,128)(2,1)S(1)} all-to-all(bf16[4,256,512]{1,2,0:T(8,128)(2,1)S(1)} %broadcast_in_dim.2), channel_id=1, replica_groups=mesh['sp'=64,'tp'=4] {'tp'}, dimensions={0} | all-to-all | bytes 2097152 | tf_op jit(solution)/shard_map/all_to_all | solution.py:372
  172.1 11.3 %convolution_convert_fusion.1 = bf16[256,2048]{1,0:T(8,128)(2,1)} fusion(bf16[2048,2048]{1,0:T(8,128)(2,1)} %bitcast.69, bf16[256,2048]{0,1:T(8,128)(2,1)S(1)} %bitcast.58, bf16[2048,2048]{1,0:T(8,128)(2,1)} %bitcast.68), kind=kOutput, calls=%fused_computation.4 | convolution fusion | flops 4297064448 | bytes 18874368 | tf_op jit(solution)/shard_map/dot_general | solution.py:417
  183.4 1.3 copy.38
  184.7 13.6 %all_to_all.16 = bf16[4,256,512]{2,1,0:T(8,128)(2,1)S(1)} all-to-all(bf16[4,256,512]{2,1,0:T(8,128)(2,1)S(1)} %bitcast.57), channel_id=1, replica_groups=mesh['sp'=64,'tp'=4] {'tp'}, dimensions={0} | all-to-all | bytes 2097152 | tf_op jit(solution)/shard_map/all_to_all | solution.py:360
  198.3 0.1 convert_reduce_fusion
  198.5 0.8 fusion.7
  (10 shorter events, 0.2 us)
Async XLA Ops:
  0.0 128.3 %copy-start = (bf16[512,2048]{1,0:T(8,128)(2,1)S(1)}, bf16[512,2048]{1,0:T(8,128)(2,1)}, u32[]{:S(2)}) copy-start(bf16[512,2048]{1,0:T(8,128)(2,1)} %param.16) | copy-start | bytes 6291460
  0.0 5.0 %copy-start.1 = (bf16[256,128]{1,0:T(8,128)(2,1)S(1)}, bf16[256,128]{1,0:T(8,128)(2,1)}, u32[]{:S(2)}) copy-start(bf16[256,128]{1,0:T(8,128)(2,1)} %param.12) | copy-start | bytes 196612
  130.1 19.0 %all-to-all-start = ((bf16[4,256,512]{2,1,0:T(8,128)(2,1)}), bf16[4,256,512]{2,1,0:T(8,128)(2,1)S(1)}, u32[]{:S(2)}, u32[]{:S(2)}) async-start(bf16[4,256,512]{2,1,0:T(8,128)(2,1)} %bitcast.55), calls=%async_computation | async-start | bytes 2097152 | tf_op jit(solution)/shard_map/all_to_all | solution.py:360

commit v2 on v1

v2 whole, which is shorter than its diff:
```python
import math

import jax
import jax.numpy as jnp
from jax import lax
from jax.experimental import pallas as pl
from jax.experimental.pallas import tpu as pltpu
from jax.sharding import PartitionSpec as P

HD = 64
GRID_W = 64
EPSILON = 1e-06
NX, NZ, NY, NC = 4, 8, 4, 2
SCALE = math.log2(math.e) / math.sqrt(HD)
MESH = pl.DeviceIdType.MESH


def prepare(projected, gain_vec, offset):
    row_count = projected.shape[0]
    head_count = projected.shape[1] // HD
    widened = projected.astype(jnp.float32).reshape(row_count, head_count, HD)
    widened = (
        widened
        * lax.rsqrt(jnp.mean(widened * widened, axis=-1, keepdims=True) + EPSILON)
        * gain_vec
    )
    position = offset + jnp.arange(row_count, dtype=jnp.int32)
    grid_row = (position // GRID_W).astype(jnp.float32)
    grid_col = (position % GRID_W).astype(jnp.float32)
    half_dim = HD // 2
    inverse = 1.0 / jnp.power(10000.0, jnp.arange(0, half_dim, 2, dtype=jnp.float32) / half_dim)
    angle = jnp.concatenate([grid_row[:, None] * inverse, grid_col[:, None] * inverse], axis=-1)
    cosine = jnp.cos(angle)[:, None, :]
    sine_table = jnp.sin(angle)[:, None, :]
    paired = widened.reshape(row_count, head_count, half_dim, 2)
    former = paired[..., 0]
    latter = paired[..., 1]
    rotated = jnp.stack(
        [former * cosine - latter * sine_table, former * sine_table + latter * cosine], axis=-1
    )
    return rotated.reshape(row_count, head_count, HD).astype(jnp.bfloat16)


class Place:
    def __init__(self):
        me = lax.axis_index("sp")
        self.core = lax.rem(me, NC)
        self.y = lax.rem(me // NC, NY)
        self.z = me // (NC * NY)
        self.x = lax.axis_index("tp")

    def yat(self, d):
        return lax.rem(self.y + (d + NY) % NY, NY)

    def xat(self, d):
        return lax.rem(self.x + (d + NX) % NX, NX)

    def dev(self, dz=0, dy=0):
        return {"sp": (lax.rem(self.z + (dz + NZ) % NZ, NZ) * NY + self.yat(dy)) * NC + self.core}

    def other(self):
        return {"sp": (self.z * NY + self.y) * NC + 1 - self.core}

    def along(self, dx):
        return {"tp": self.xat(dx)}


class Mail:
    def __init__(self, place, send_sems, recv_sems):
        self.at, self.ss, self.rs, self.sent = place, send_sems, recv_sems, []

    def copy(self, key, src, dst, target):
        return pltpu.make_async_remote_copy(
            src_ref=src,
            dst_ref=dst,
            send_sem=self.ss.at[key],
            recv_sem=self.rs.at[key],
            device_id=target,
            device_id_type=MESH,
        )

    def send(self, key, src, dst, target):
        self.copy(key, src(), dst(), target()).start()
        self.sent.append((key, src, dst, target))

    def got(self, key, ref):
        self.copy(key, ref, ref, self.at.other()).wait_recv()

    def finish(self):
        for key, src, dst, target in self.sent:
            self.copy(key, src(), dst(), target()).wait_send()


class Around(Mail):
    SEMS = 7

    def __init__(self, own, buf, half, *rest):
        super().__init__(*rest)
        self.own, self.buf, self.half = own, buf, half

    def slot(self, k):
        return self.buf.at[k, self.at.core]

    def part(self, k, second):
        return self.buf.at[k, self.at.core, pl.ds(self.half if second else 0, self.half)]

    def over(self, k):
        self.send(3 + k, lambda: self.slot(k), lambda: self.slot(k), self.at.other)

    def s1(self):
        own = lambda: self.own.at[self.at.core]
        self.send(0, own, lambda: self.slot(1), lambda: self.at.along(1))
        self.send(1, own, lambda: self.slot(2), lambda: self.at.along(-1))

    def s2(self):
        self.got(0, self.slot(1))
        self.send(2, lambda: self.part(1, False), lambda: self.part(3, False), lambda: self.at.along(1))
        self.got(1, self.slot(2))
        self.send(3, lambda: self.part(2, True), lambda: self.part(3, True), lambda: self.at.along(-1))
        self.over(1)
        self.over(2)

    def s3(self):
        self.got(2, self.part(3, False))
        self.got(3, self.part(3, True))
        self.over(3)

    def w(self):
        for k in (1, 2, 3):
            self.got(3 + k, self.buf.at[k, 1 - self.at.core])


class ZFirst(Mail):
    SEMS = 33

    def __init__(self, own, buf, half, *rest):
        super().__init__(*rest)
        self.own, self.buf, self.half = own, buf, half

    def slot(self, k):
        return self.buf.at[k, self.at.y, self.at.core]

    def part(self, k, dy, second):
        return self.buf.at[k, self.at.yat(dy), self.at.core, pl.ds(self.half if second else 0, self.half)]

    def slots(self, d):
        return pl.ds(0, 1) if d == 0 else pl.ds(7, 1) if d == 4 else pl.ds(2 * d - 1, 2)

    def pair(self, d, dy=0):
        return self.buf.at[self.slots(d), self.at.yat(dy), self.at.core]

    def columns(self, d, other=False):
        core = 1 - self.at.core if other else self.at.core
        return self.buf.at[self.slots(d), :, core]

    def along_y(self, d):
        self.send(8 + d, lambda: self.pair(d), lambda: self.pair(d), lambda: self.at.dev(0, 1))
        self.send(13 + d, lambda: self.pair(d), lambda: self.pair(d), lambda: self.at.dev(0, -1))

    def a(self, d):
        if d == 0:
            self.send(8, lambda: self.own, lambda: self.slot(0), lambda: self.at.dev(0, 1))
            self.send(13, lambda: self.own, lambda: self.slot(0), lambda: self.at.dev(0, -1))
            self.send(0, lambda: self.own, lambda: self.slot(2), lambda: self.at.dev(1))
            self.send(4, lambda: self.own, lambda: self.slot(1), lambda: self.at.dev(-1))
            return
        if d == 4:
            self.got(3, self.part(7, 0, False))
            self.got(7, self.part(7, 0, True))
        else:
            low, high = 2 * d, 2 * d - 1
            self.got(d - 1, self.slot(low))
            if d < 3:
                self.send(d, lambda: self.slot(low), lambda: self.slot(low + 2), lambda: self.at.dev(1))
            else:
                self.send(3, lambda: self.part(6, 0, False), lambda: self.part(7, 0, False), lambda: self.at.dev(1))
            self.got(3 + d, self.slot(high))
            if d < 3:
                self.send(4 + d, lambda: self.slot(high), lambda: self.slot(high + 2), lambda: self.at.dev(-1))
            else:
                self.send(7, lambda: self.part(5, 0, True), lambda: self.part(7, 0, True), lambda: self.at.dev(-1))
        self.along_y(d)

    def piece(self, d, dy, second):
        if d in (0, 4):
            return self.part(0 if d == 0 else 7, dy, second)
        return self.buf.at[2 * d if second else 2 * d - 1, self.at.yat(dy), self.at.core]

    def b(self, d):
        self.got(8 + d, self.pair(d, -1))
        one = lambda: self.piece(d, -1, False)
        self.send(18 + d, one, one, lambda: self.at.dev(0, 1))
        self.got(13 + d, self.pair(d, 1))
        two = lambda: self.piece(d, 1, True)
        self.send(23 + d, two, two, lambda: self.at.dev(0, -1))

    def c(self, d):
        self.got(18 + d, self.piece(d, 2, False))
        self.got(23 + d, self.piece(d, 2, True))
        self.send(28 + d, lambda: self.columns(d), lambda: self.columns(d), self.at.other)

    def w(self, d):
        self.got(28 + d, self.columns(d, True))


class YFirst(Mail):
    SEMS = 17

    def __init__(self, own, buf, half, *rest):
        super().__init__(*rest)
        self.own, self.buf, self.half = own, buf, half

    def slot(self, dy):
        return self.buf.at[0, self.at.yat(dy), self.at.core]

    def part(self, dy, second):
        return self.slot(dy).at[pl.ds(self.half if second else 0, self.half)]

    def column(self, k):
        return self.buf.at[k, :, self.at.core]

    def two(self, k, second):
        return self.buf.at[k, pl.ds(2 if second else 0, 2), self.at.core]

    def columns(self, d, other=False):
        core = 1 - self.at.core if other else self.at.core
        return self.buf.at[pl.ds(0, 1) if d == 0 else pl.ds(7, 1) if d == 4 else pl.ds(2 * d - 1, 2), :, core]

    def over(self, d):
        self.send(12 + d, lambda: self.columns(d), lambda: self.columns(d), self.at.other)

    def s1(self):
        self.send(0, lambda: self.own, lambda: self.slot(0), lambda: self.at.dev(0, 1))
        self.send(1, lambda: self.own, lambda: self.slot(0), lambda: self.at.dev(0, -1))

    def s2(self):
        self.got(0, self.slot(-1))
        one = lambda: self.part(-1, False)
        self.send(2, one, one, lambda: self.at.dev(0, 1))
        self.got(1, self.slot(1))
        two = lambda: self.part(1, True)
        self.send(3, two, two, lambda: self.at.dev(0, -1))

    def s3(self):
        self.got(2, self.part(2, False))
        self.got(3, self.part(2, True))
        self.send(4, lambda: self.column(0), lambda: self.column(2), lambda: self.at.dev(1))
        self.send(8, lambda: self.column(0), lambda: self.column(1), lambda: self.at.dev(-1))
        self.over(0)

    def z(self, d):
        if d == 4:
            self.got(7, self.two(7, False))
            self.got(11, self.two(7, True))
            self.over(4)
            return
        low, high = 2 * d, 2 * d - 1
        self.got(3 + d, self.column(low))
        if d < 3:
            self.send(4 + d, lambda: self.column(low), lambda: self.column(low + 2), lambda: self.at.dev(1))
        else:
            self.send(7, lambda: self.two(6, False), lambda: self.two(7, False), lambda: self.at.dev(1))
        self.got(7 + d, self.column(high))
        if d < 3:
            self.send(8 + d, lambda: self.column(high), lambda: self.column(high + 2), lambda: self.at.dev(-1))
        else:
            self.send(11, lambda: self.two(5, True), lambda: self.two(7, True), lambda: self.at.dev(-1))
        self.over(d)

    def w(self):
        for d in range(5):
            self.got(12 + d, self.columns(d, True))


def attend(kv, q_ref, s_scr, acc, peak, zs, h):
    tiles, width = 4, 256
    where = [(y, c) for y in range(NY) for c in range(NC)]

    def scores(j):
        top = None
        for a, (y, c) in enumerate(where):
            t = jnp.dot(
                kv[zs, y, c, 0:256, :],
                q_ref[h, :, j * width : (j + 1) * width],
                preferred_element_type=jnp.float32,
            )
            s_scr[j % 2, a * 256 : (a + 1) * 256, :] = t
            t = jnp.max(t.reshape(32, 8, width), axis=0)
            top = t if top is None else jnp.maximum(top, t)
        return top

    ones = jnp.ones((16, 256), jnp.bfloat16)
    later = scores(0)
    for j in range(tiles):
        top = later
        if j + 1 < tiles:
            later = scores(j + 1)
        cols = slice(j * width, (j + 1) * width)
        before = peak[h, 0:1, cols]
        now = jnp.maximum(before, jnp.max(top, axis=0, keepdims=True) * SCALE)
        peak[h, 0:1, cols] = now
        rescale = jnp.exp2(before - now)
        added = None
        for a, (y, c) in enumerate(where):
            exps = jnp.exp2(s_scr[j % 2, a * 256 : (a + 1) * 256, :] * SCALE - now)
            first = kv[zs, y, c, pl.ds(pl.multiple_of(256 + h * HD, HD), HD), :]
            second = kv[zs, y, c, pl.ds(pl.multiple_of(384 + h * HD, HD), HD), :]
            left = jnp.concatenate([jnp.concatenate([first, second], axis=1), ones], axis=0)
            term = jnp.dot(left, exps.astype(jnp.bfloat16), preferred_element_type=jnp.float32)
            added = term if added is None else added + term
        acc[h, :, cols] = acc[h, :, cols] * rescale + added


def layer_kernel(
    q_ref, kv_in, up_in, down_in, ow_in, stream, gain, o_ref,
    kv, up, down, ow, s_scr, acc, peak, st, heads, mid, nrm, hid, part, arrived, transit,
    kv_s, kv_r, up_s, up_r, down_s, down_r, ow_s, ow_r, tp_s, tp_r, own_sem,
):
    at = Place()
    own = [
        pltpu.make_async_copy(src, dst, own_sem.at[k])
        for k, (src, dst) in enumerate(
            (
                (kv_in, kv.at[0, at.y, at.core]),
                (up_in, up.at[0, at.y, at.core]),
                (down_in, down.at[0, at.y, at.core]),
                (ow_in, ow.at[0]),
                (stream.at[at.x], st),
            )
        )
    ]
    for copy in own:
        copy.start()
    barrier = pltpu.get_barrier_semaphore()
    nearby = [at.dev(1), at.dev(-1), at.dev(0, 1), at.dev(0, -1), at.other()]
    nearby += [at.along(1), at.along(-1), at.along(2)]
    for near in nearby:
        pl.semaphore_signal(barrier, inc=1, device_id=near, device_id_type=MESH)
    acc[...] = jnp.zeros_like(acc)
    peak[...] = jnp.full_like(peak, -1e30)
    pl.semaphore_wait(barrier, len(nearby))
    pairs = ZFirst(kv_in, kv, 256, at, kv_s, kv_r)
    ups = YFirst(up_in, up, 16, at, up_s, up_r)
    downs = ZFirst(down_in, down, 16, at, down_s, down_r)
    outs = Around(ow_in, ow, 128, at, ow_s, ow_r)
    across = Mail(at, tp_s, tp_r)

    pairs.a(0)
    ups.s1()
    outs.s1()
    own[0].wait()
    pairs.b(0)
    pairs.a(1)
    pairs.c(0)
    pairs.w(0)
    polls = {
        1: (lambda: pairs.b(1), lambda: pairs.a(2), ups.s2),
        2: (lambda: pairs.c(1), own[1].wait, ups.s3, lambda: pairs.w(1)),
        4: (lambda: pairs.b(2), lambda: pairs.a(3)),
        5: (lambda: pairs.c(2), lambda: pairs.a(4), lambda: downs.a(0)),
        6: (lambda: pairs.w(2), lambda: ups.z(1), lambda: downs.a(1)),
        7: (lambda: pairs.b(3),),
        8: (lambda: pairs.c(3), lambda: pairs.b(4), lambda: downs.a(2)),
        9: (lambda: pairs.c(4), lambda: downs.b(0), outs.s2),
        10: (lambda: pairs.w(3), lambda: ups.z(2), lambda: downs.b(1), own[2].wait, lambda: downs.c(0)),
        11: (lambda: downs.a(3),),
        12: (lambda: downs.b(2), lambda: downs.c(1)),
        13: (lambda: downs.a(4), outs.s3),
        14: (lambda: pairs.w(4), lambda: ups.z(3)),
        15: (lambda: downs.b(3), lambda: downs.c(2)),
    }

    def step(n, carry):
        for k, todo in polls.items():

            @pl.when(n == k)
            def _(todo=todo):
                for do in todo:
                    do()

        attend(kv, q_ref, s_scr, acc, peak, n // 2, lax.rem(n, 2))
        return carry

    lax.fori_loop(0, 2 * NZ, step, 0)

    for k in range(4):
        sides = []
        for g in (2 * k, 2 * k + 1):
            h, cols = g // 4, slice(g % 4 * 256, (g % 4 + 1) * 256)
            sides.append(jnp.transpose(acc[h, 0:HD, cols] / acc[h, HD : HD + 1, cols]))
        both = jnp.concatenate(sides, axis=1).astype(jnp.bfloat16)
        heads[0, :, :, k * 128 : (k + 1) * 128] = both.reshape(NX, 64, 128)
    offsets = (0, -1, 1, 2)
    own[3].wait()
    own[4].wait()
    outs.w()
    across.send(2, lambda: heads.at[0, at.xat(2)], lambda: heads.at[1, 2], lambda: at.along(2))
    across.send(0, lambda: heads.at[0, at.xat(1)], lambda: heads.at[1, 0], lambda: at.along(1))
    across.send(1, lambda: heads.at[0, at.xat(-1)], lambda: heads.at[1, 1], lambda: at.along(-1))
    downs.b(4)
    downs.c(3)
    for k in range(3):
        across.got(k, heads.at[1, k])
    lefts = [heads[0, at.x], heads[1, 0], heads[1, 1], heads[1, 2]]
    for j in range(5):
        if j < 4:
            cols = slice(j * 512, (j + 1) * 512)
            attended = None
            for i, left in enumerate(lefts):
                term = jnp.dot(left[:, 0:256], ow[i, 0, :, cols], preferred_element_type=jnp.float32)
                term += jnp.dot(left[:, 256:512], ow[i, 1, :, cols], preferred_element_type=jnp.float32)
                term = term.astype(jnp.bfloat16).astype(jnp.float32)
                attended = term if attended is None else attended + term
            mid[at.x, j] = (st[:, cols].astype(jnp.float32) + attended).astype(jnp.bfloat16)
        if j > 0:
            chunk = lambda j=j: mid.at[at.x, j - 1]
            across.send(3 + j - 1, chunk, chunk, lambda: at.along(1))
            across.send(7 + j - 1, chunk, chunk, lambda: at.along(-1))

    def norm(i):
        rows = jnp.concatenate([mid[at.xat(offsets[i]), j] for j in range(4)], axis=1)
        rows = rows.astype(jnp.float32)
        mean = jnp.mean(rows * rows, axis=-1, keepdims=True)
        nrm[i * 64 : (i + 1) * 64, :] = (rows * lax.rsqrt(mean + EPSILON) * gain[...]).astype(jnp.bfloat16)

    def slot_z(k):
        return at.z if k == 0 else lax.rem(at.z + (4 if k == 7 else (k + 1) // 2 if k % 2 else NZ - k // 2), NZ)

    def lift(first, last):
        rows = slice(first * 64, last * 64)
        for t in range(4):
            cols = slice(t * 512, (t + 1) * 512)
            sums = None
            for k in range(NZ):
                left = nrm[rows, pl.ds(pl.multiple_of(slot_z(k) * 256, 256), 256)]
                term = jnp.dot(left, up[k, :, :, :, cols].reshape(256, 512), preferred_element_type=jnp.float32)
                sums = term if sums is None else sums + term
            hid[rows, cols] = jnp.square(jnp.maximum(sums, 0.0)).astype(jnp.bfloat16)

    norm(0)
    for j in (0, 1):
        chunk = lambda j=j: mid.at[at.xat(-1), j]
        across.got(3 + j, chunk())
        across.send(11 + j, chunk, chunk, lambda: at.along(1))
    for j in (2, 3):
        chunk = lambda j=j: mid.at[at.xat(1), j]
        across.got(7 + j, chunk())
        across.send(11 + j, chunk, chunk, lambda: at.along(-1))
    ups.z(4)
    downs.c(4)
    ups.w()
    lift(0, 1)
    for j in (2, 3):
        across.got(3 + j, mid.at[at.xat(-1), j])
    for j in (0, 1):
        across.got(7 + j, mid.at[at.xat(1), j])
    norm(1)
    norm(2)
    lift(1, 3)
    for j in range(4):
        across.got(11 + j, mid.at[at.xat(2), j])
    norm(3)
    lift(3, 4)
    for d in range(5):
        downs.w(d)

    def lower(k):
        for t in range(2):
            r = lax.rem(2 * at.xat(k) + t + NZ - at.z, NZ)
            where = jnp.where(r > 4, 2 * (NZ - r), jnp.maximum(2 * r - 1, 0))
            sums = lax.dot_general(
                hid[...],
                down[where].reshape(256, 2048),
                (((1,), (1,)), ((), ())),
                preferred_element_type=jnp.float32,
            ).astype(jnp.bfloat16)
            for i in range(4):
                part[k, at.xat(offsets[i]), :, t * 256 : (t + 1) * 256] = sums[i * 64 : (i + 1) * 64]

    lower(2)
    lower(1)
    across.send(15, lambda: part.at[2, pl.ds(0, 2)], lambda: transit.at[0], lambda: at.along(1))
    across.send(16, lambda: part.at[2, pl.ds(2, 2)], lambda: transit.at[1], lambda: at.along(-1))
    lower(3)
    across.send(17, lambda: part.at[1], lambda: arrived.at[0], lambda: at.along(1))
    lower(0)
    across.send(18, lambda: part.at[3], lambda: arrived.at[1], lambda: at.along(-1))
    across.got(15, transit.at[0])
    across.send(19, lambda: transit.at[0], lambda: arrived.at[2, pl.ds(0, 2)], lambda: at.along(1))
    across.got(16, transit.at[1])
    across.send(20, lambda: transit.at[1], lambda: arrived.at[2, pl.ds(2, 2)], lambda: at.along(-1))
    across.got(17, arrived.at[0])
    across.got(18, arrived.at[1])
    across.got(19, arrived.at[2, pl.ds(0, 2)])
    across.got(20, arrived.at[2, pl.ds(2, 2)])
    for s in range(4):
        total = part[0, s].astype(jnp.float32)
        for k in range(3):
            total += arrived[k, s].astype(jnp.float32)
        o_ref[s] = (mid[s, at.x].astype(jnp.float32) + total).astype(jnp.bfloat16)
    for mail in (pairs, ups, downs, outs, across):
        mail.finish()


def layer(*operands):
    anywhere = pl.BlockSpec(memory_space=pl.ANY)
    vmem = pl.BlockSpec(memory_space=pltpu.VMEM)
    bf16, f32 = jnp.bfloat16, jnp.float32
    held = [
        ((NZ, NY, NC, 512, 128), bf16),
        ((NZ, NY, NC, 32, 2048), bf16),
        ((NZ, NY, NC, 32, 2048), bf16),
        ((NX, 2, 256, 2048), bf16),
        ((2, 2048, 256), f32),
        ((2, 80, 1024), f32),
        ((2, 8, 1024), f32),
        ((64, 2048), bf16),
        ((2, NX, 64, 512), bf16),
        ((NX, 4, 64, 512), bf16),
        ((256, 2048), bf16),
        ((256, 2048), bf16),
        ((NX, NX, 64, 512), bf16),
        ((3, NX, 64, 512), bf16),
        ((2, 2, 64, 512), bf16),
    ]
    counts = (33, 33, 17, 17, 33, 33, 7, 7, 21, 21, 5)
    return pl.pallas_call(
        layer_kernel,
        name="layer",
        out_shape=jax.ShapeDtypeStruct((NX, 64, 512), bf16),
        in_specs=[vmem, anywhere, anywhere, anywhere, anywhere, anywhere, vmem],
        out_specs=vmem,
        scratch_shapes=[
            *(pltpu.VMEM(shape, kind) for shape, kind in held),
            *(pltpu.SemaphoreType.DMA((n,)) for n in counts),
        ],
        compiler_params=pltpu.CompilerParams(
            collective_id=0, has_side_effects=True, vmem_limit_bytes=60 * 1024 * 1024
        ),
    )(*operands)


def shards(
    queries,
    keys,
    values,
    query_gain,
    key_gain,
    stream,
    out_weight,
    mixer_gain,
    up_weight,
    down_weight,
):
    rows = queries.shape[0]
    offset = lax.axis_index("sp") * rows
    pq = prepare(queries, query_gain, offset)
    pq = jnp.transpose(pq.reshape(rows, 2, 4, HD), (1, 3, 2, 0)).reshape(2, HD, 4 * rows)
    none = jnp.zeros((1, HD, 4 * rows), jnp.bfloat16)
    q_wide = jnp.concatenate(
        [jnp.concatenate([pq[:1], none], axis=1), jnp.concatenate([none, pq[1:]], axis=1)], axis=0
    )
    pk = prepare(keys, key_gain, offset).reshape(rows, 128)
    v_turned = jnp.transpose(values.reshape(2, 128, 128), (0, 2, 1)).reshape(256, 128)
    kv_block = jnp.concatenate([pk, v_turned], axis=0)
    out_block = out_weight.reshape(2, 256, -1)
    width = stream.shape[1]
    updated = layer(
        q_wide,
        kv_block,
        up_weight,
        down_weight.T,
        out_block,
        stream.reshape(NX, rows // NX, width),
        mixer_gain.reshape(1, width),
    )
    return updated.reshape(rows, -1)


def solution(mesh):
    return jax.shard_map(
        shards,
        mesh=mesh,
        in_specs=(
            P("sp", "tp"),
            P("sp", "tp"),
            P("sp", "tp"),
            P(),
            P(),
            P("sp", None),
            P("tp", None),
            P(),
            P("sp", "tp"),
            P("tp", "sp"),
        ),
        out_specs=P("sp", "tp"),
        check_vma=False,
    )
```

time: 202 us -> 147 us (0.73); the launches traced: 199 us -> 147 us
  blocking collectives: 35 us -> 0 us
  Pallas kernels: 119 us -> 139 us
  waiting for transfers between devices: 14.2 us -> 0 us
  matrix products: 12 us -> 0 us
  local copies, waits for them, and re-layouts: 8.76 us -> 4.45 us
  starting transfers between devices: 4.01 us -> 0 us
  other arithmetic: 6.16 us -> 3.84 us
    all_to_all x2 -> x0, blocking collectives: 28.2 us -> none  [the longest x1 14.5 us: gather_directly(): lax.all_to_all(copies, axis, split_axis=0, concat_axis=0, tiled=True)]
    pallas_call x1, Pallas kernels: 119 us -> 139 us  [layer(): pl.pallas_call(layer_kernel, name='layer', out_shape=jax.ShapeDtypeStruct...]
    all_to_all x1 -> x0, waiting for transfers between devices: 14.2 us -> none  [sum_at_owner(): lax.all_to_all(pieces, axis, split_axis=0, concat_axis=0, tiled=True)]
    dot_general x2 -> x0, matrix products: 12 us -> none  [the longest x1 11.3 us: shards(): lax.dot_general(hidden, down_turned, (((1,), (1,)), ((), ())), preferred_...]
    psum x1 -> x0, blocking collectives: 6.88 us -> none  [shards(): squares = lax.psum(jnp.sum(own_wide * own_wide, axis=-1), 'tp')]
    all_to_all x1 -> x0, starting transfers between devices: 4.01 us -> none  [sum_at_owner(): lax.all_to_all(pieces, axis, split_axis=0, concat_axis=0, tiled=True)]
    reshape x3 -> x0, local copies, waits for them, and re-layouts: 3.37 us -> none  [the longest x2 2.4 us: in_blocks(): pieces = x.reshape(*dims[:dim], count, dims[dim] // count, *dims[dim + 1:])]
  transfers between devices with their start and end apart: 1 -> 0, of which waited for: 1 -> 0; matrix products, arithmetic and copies ran while one was open for 0% -> 0% of each run, Pallas kernels for 0% -> 0%
where the time goes in v2:
time: 147 us
  Pallas kernels  139 us (95%)
  local copies, waits for them, and re-layouts  4.45 us (3%)
  other arithmetic  3.84 us (3%)
    pallas_call x1, Pallas kernels, layer(): pl.pallas_call(layer_kernel, name='layer', out_shape=jax.ShapeDtypeStruct...  139 us

profile of v2, /device:TPU:1, one launch (start us, length us, event | category | flops | bytes accessed | tf_op | source)
XLA Modules:
  0.0 147.0 jit_solution(5165700976299945085)
XLA Ops:
  0.0 0.1 broadcast_multiply_fusion.1
  0.1 0.1 fusion.4
  0.2 1.1 copy.12
  1.3 0.3 reshape.157
  1.6 0.1 bitcast_reduce_fusion
  1.7 0.8 mul.172
  2.4 0.3 multiply_multiply_fusion
  2.7 0.0 copy-start
  2.7 0.0 copy-start.2
  2.7 0.7 subtract_convert_fusion
  3.4 0.6 pad_maximum_fusion
  4.0 0.0 copy-start.1
  4.0 0.1 convert_element_type.35
  4.2 0.8 fusion.2.q_ref
  5.1 0.0 copy-done
  5.1 0.1 copy.15
  5.2 0.1 reshape.158
  5.3 0.0 copy-done.2
  5.3 0.1 mul.191
  5.4 0.1 multiply_multiply_fusion.1
  5.5 0.2 subtract_convert_fusion.1
  5.7 0.2 pad_maximum_fusion.2
  5.9 0.1 copy.17
  6.0 0.0 copy-done.1
  6.0 0.1 copy.16
  6.2 0.7 pad_maximum_fusion.1.kv_in
  6.8 138.5 %layer.1 = bf16[4,64,512]{2,1,0:T(8,128)(2,1)} custom-call(bf16[2,128,1024]{2,1,0:T(8,128)(2,1)} %fusion.2.q_ref, bf16[512,128]{1,0:T(8,128)(2,1)} %pad_maximum_fusion.1.kv_in, bf16[32,2048]{1,0:T(8,128)(2,1)} %up_in.1, bf16[32,2048]{1,0:T(8,128)(2,1)} %bitcast.35, bf16[2,256,2048]{2,1,0:T(8,128)(2,1)} %bitcast.28, bf16[4,64,2048]{2,1,0:T(8,128)(2,1)} %bitcast.31, ...), custom_call_target="tpu_custom_call" | custom-call | tf_op jit(solution)/shard_map/layer/pallas_call | solution.py:527
  145.4 1.7 %copy.21 = bf16[256,512]{1,0:T(8,128)(2,1)} copy(bf16[256,512]{1,0:T(8,128)(2,1)} %bitcast.29) | data formatting | bytes 524288
  (9 shorter events, 0.1 us)
Async XLA Ops:
  2.7 2.3 %copy-start = (bf16[256,128]{1,0:T(8,128)(2,1)S(1)}, bf16[256,128]{1,0:T(8,128)(2,1)}, u32[]{:S(2)}) copy-start(bf16[256,128]{1,0:T(8,128)(2,1)} %param.11) | copy-start | bytes 196612
  2.7 2.6 %copy-start.2 = (f32[64]{0:T(128)S(1)}, f32[64]{0:T(128)}, u32[]{:S(2)}) copy-start(f32[64]{0:T(128)} %param.14) | copy-start | bytes 772
  4.0 2.0 %copy-start.1 = (bf16[256,128]{1,0:T(8,128)(2,1)S(1)}, bf16[256,128]{1,0:T(8,128)(2,1)}, u32[]{:S(2)}) copy-start(bf16[256,128]{1,0:T(8,128)(2,1)} %param.12) | copy-start | bytes 196612

commit v3 on v2

--- a/solution.py
+++ b/solution.py
@@ -313,7 +313,7 @@
 
 def layer_kernel(
     q_ref, kv_in, up_in, down_in, ow_in, stream, gain, o_ref,
-    kv, up, down, ow, s_scr, acc, peak, st, heads, mid, nrm, hid, part, arrived, transit,
+    kv, up, down, ow, s_scr, acc, peak, st, heads, mid, nrm, hid, part, arrived, transit, joined,
     kv_s, kv_r, up_s, up_r, down_s, down_r, ow_s, ow_r, tp_s, tp_r, own_sem,
 ):
     at = Place()
@@ -348,36 +348,48 @@
     pairs.a(0)
     ups.s1()
     outs.s1()
+    pairs.a(1)
+    pairs.b(0)
+    ups.s2()
+    pairs.b(1)
+    pairs.a(2)
     own[0].wait()
-    pairs.b(0)
-    pairs.a(1)
     pairs.c(0)
+    downs.a(0)
+    own[1].wait()
+    ups.s3()
     pairs.w(0)
     polls = {
-        1: (lambda: pairs.b(1), lambda: pairs.a(2), ups.s2),
-        2: (lambda: pairs.c(1), own[1].wait, ups.s3, lambda: pairs.w(1)),
-        4: (lambda: pairs.b(2), lambda: pairs.a(3)),
-        5: (lambda: pairs.c(2), lambda: pairs.a(4), lambda: downs.a(0)),
-        6: (lambda: pairs.w(2), lambda: ups.z(1), lambda: downs.a(1)),
+        1: (lambda: pairs.c(1),),
+        2: (lambda: pairs.w(1),),
+        3: (lambda: pairs.b(2), lambda: pairs.a(3), lambda: downs.a(1),),
+        4: (outs.s2,),
+        5: (lambda: pairs.c(2),),
+        6: (lambda: pairs.w(2), lambda: ups.z(1),),
         7: (lambda: pairs.b(3),),
-        8: (lambda: pairs.c(3), lambda: pairs.b(4), lambda: downs.a(2)),
-        9: (lambda: pairs.c(4), lambda: downs.b(0), outs.s2),
-        10: (lambda: pairs.w(3), lambda: ups.z(2), lambda: downs.b(1), own[2].wait, lambda: downs.c(0)),
-        11: (lambda: downs.a(3),),
-        12: (lambda: downs.b(2), lambda: downs.c(1)),
-        13: (lambda: downs.a(4), outs.s3),
-        14: (lambda: pairs.w(4), lambda: ups.z(3)),
-        15: (lambda: downs.b(3), lambda: downs.c(2)),
+        8: (lambda: pairs.a(4), lambda: downs.b(0), lambda: downs.a(2),),
+        9: (lambda: pairs.c(3), outs.s3,),
+        10: (lambda: pairs.b(4), lambda: downs.b(1), lambda: ups.z(2), lambda: pairs.w(3),),
+        13: (lambda: downs.a(3), lambda: pairs.c(4),),
+        14: (lambda: pairs.w(4),),
+        15: (lambda: downs.b(2), lambda: ups.z(3),),
     }
 
     def step(n, carry):
-        for k, todo in polls.items():
-
-            @pl.when(n == k)
-            def _(todo=todo):
-                for do in todo:
-                    do()
-
+        def poll(keys):
+            if len(keys) == 1:
+
+                @pl.when(n == keys[0])
+                def _():
+                    for do in polls[keys[0]]:
+                        do()
+
+            else:
+                at_half = len(keys) // 2
+                pl.when(n < keys[at_half])(lambda: poll(keys[:at_half]))
+                pl.when(n >= keys[at_half])(lambda: poll(keys[at_half:]))
+
+        poll(sorted(polls))
         attend(kv, q_ref, s_scr, acc, peak, n // 2, lax.rem(n, 2))
         return carry
 
@@ -397,8 +409,11 @@
     across.send(2, lambda: heads.at[0, at.xat(2)], lambda: heads.at[1, 2], lambda: at.along(2))
     across.send(0, lambda: heads.at[0, at.xat(1)], lambda: heads.at[1, 0], lambda: at.along(1))
     across.send(1, lambda: heads.at[0, at.xat(-1)], lambda: heads.at[1, 1], lambda: at.along(-1))
-    downs.b(4)
-    downs.c(3)
+    own[2].wait()
+    downs.c(0)
+    downs.a(4)
+    downs.b(3)
+    downs.c(1)
     for k in range(3):
         across.got(k, heads.at[1, k])
     lefts = [heads[0, at.x], heads[1, 0], heads[1, 1], heads[1, 2]]
@@ -446,9 +461,14 @@
         chunk = lambda j=j: mid.at[at.xat(1), j]
         across.got(7 + j, chunk())
         across.send(11 + j, chunk, chunk, lambda: at.along(-1))
+    downs.b(4)
     ups.z(4)
+    downs.c(2)
+    ups.w()
+    downs.w(1)
+    downs.w(0)
     downs.c(4)
-    ups.w()
+    downs.c(3)
     lift(0, 1)
     for j in (2, 3):
         across.got(3 + j, mid.at[at.xat(-1), j])
@@ -461,8 +481,9 @@
         across.got(11 + j, mid.at[at.xat(2), j])
     norm(3)
     lift(3, 4)
-    for d in range(5):
-        downs.w(d)
+    downs.w(3)
+    downs.w(2)
+    downs.w(4)
 
     def lower(k):
         for t in range(2):
@@ -479,25 +500,32 @@
 
     lower(2)
     lower(1)
-    across.send(15, lambda: part.at[2, pl.ds(0, 2)], lambda: transit.at[0], lambda: at.along(1))
-    across.send(16, lambda: part.at[2, pl.ds(2, 2)], lambda: transit.at[1], lambda: at.along(-1))
+    first, second = pl.ds(0, 2), pl.ds(2, 2)
+    across.send(15, lambda: part.at[2, first], lambda: transit.at[0], lambda: at.along(1))
+    across.send(16, lambda: part.at[2, second], lambda: transit.at[1], lambda: at.along(-1))
     lower(3)
-    across.send(17, lambda: part.at[1], lambda: arrived.at[0], lambda: at.along(1))
+    across.send(17, lambda: part.at[1, second], lambda: arrived.at[0, second], lambda: at.along(1))
     lower(0)
-    across.send(18, lambda: part.at[3], lambda: arrived.at[1], lambda: at.along(-1))
+    across.send(18, lambda: part.at[3, first], lambda: arrived.at[1, first], lambda: at.along(-1))
     across.got(15, transit.at[0])
-    across.send(19, lambda: transit.at[0], lambda: arrived.at[2, pl.ds(0, 2)], lambda: at.along(1))
+    for s in range(2):
+        total = part[1, s].astype(jnp.float32) + transit[0, s].astype(jnp.float32)
+        joined[0, s] = total.astype(jnp.bfloat16)
     across.got(16, transit.at[1])
-    across.send(20, lambda: transit.at[1], lambda: arrived.at[2, pl.ds(2, 2)], lambda: at.along(-1))
-    across.got(17, arrived.at[0])
-    across.got(18, arrived.at[1])
-    across.got(19, arrived.at[2, pl.ds(0, 2)])
-    across.got(20, arrived.at[2, pl.ds(2, 2)])
-    for s in range(4):
-        total = part[0, s].astype(jnp.float32)
-        for k in range(3):
+    for s in range(2):
+        total = part[3, 2 + s].astype(jnp.float32) + transit[1, s].astype(jnp.float32)
+        joined[1, s] = total.astype(jnp.bfloat16)
+    across.send(19, lambda: joined.at[0], lambda: arrived.at[0, first], lambda: at.along(1))
+    across.send(20, lambda: joined.at[1], lambda: arrived.at[1, second], lambda: at.along(-1))
+    across.got(17, arrived.at[0, second])
+    across.got(18, arrived.at[1, first])
+    across.got(19, arrived.at[0, first])
+    across.got(20, arrived.at[1, second])
+    for s in range(NX):
+        total = mid[s, at.x].astype(jnp.float32) + part[0, s].astype(jnp.float32)
+        for k in range(2):
             total += arrived[k, s].astype(jnp.float32)
-        o_ref[s] = (mid[s, at.x].astype(jnp.float32) + total).astype(jnp.bfloat16)
+        o_ref[s] = total.astype(jnp.bfloat16)
     for mail in (pairs, ups, downs, outs, across):
         mail.finish()
 
@@ -520,7 +548,8 @@
         ((256, 2048), bf16),
         ((256, 2048), bf16),
         ((NX, NX, 64, 512), bf16),
-        ((3, NX, 64, 512), bf16),
+        ((2, NX, 64, 512), bf16),
+        ((2, 2, 64, 512), bf16),
         ((2, 2, 64, 512), bf16),
     ]
     counts = (33, 33, 17, 17, 33, 33, 7, 7, 21, 21, 5)

time: 147 us -> 121 us (0.82); the launches traced: 147 us -> 120 us
  Pallas kernels: 139 us -> 111 us
    pallas_call x1, Pallas kernels: 139 us -> 111 us  [layer(): pl.pallas_call(layer_kernel, name='layer', out_shape=jax.ShapeDtypeStruct...]
where the time goes in v3:
time: 121 us; the launch traced here: 120 us
  Pallas kernels  111 us (92%)
  local copies, waits for them, and re-layouts  4.45 us (4%)
  other arithmetic  3.84 us (3%)
    pallas_call x1, Pallas kernels, layer(): pl.pallas_call(layer_kernel, name='layer', out_shape=jax.ShapeDtypeStruct...  111 us
    unnamed x10, local copies, waits for them, and re-layouts  2.9 us

profile of v3, /device:TPU:1, one launch (start us, length us, event | category | flops | bytes accessed | tf_op | source)
XLA Modules:
  0.0 119.6 jit_solution(8368798662991271535)
XLA Ops:
  0.0 0.1 broadcast_multiply_fusion.1
  0.1 0.1 fusion.4
  0.2 1.1 copy.12
  1.3 0.3 reshape.157
  1.6 0.1 bitcast_reduce_fusion
  1.7 0.8 mul.172
  2.4 0.3 multiply_multiply_fusion
  2.7 0.0 copy-start
  2.7 0.0 copy-start.2
  2.7 0.7 subtract_convert_fusion
  3.4 0.6 pad_maximum_fusion
  4.0 0.0 copy-start.1
  4.0 0.1 convert_element_type.35
  4.2 0.8 fusion.2.q_ref
  5.1 0.0 copy-done
  5.1 0.1 copy.15
  5.2 0.1 reshape.158
  5.3 0.0 copy-done.2
  5.3 0.1 mul.191
  5.4 0.1 multiply_multiply_fusion.1
  5.5 0.2 subtract_convert_fusion.1
  5.7 0.2 pad_maximum_fusion.2
  5.9 0.1 copy.17
  6.0 0.0 copy-done.1
  6.0 0.1 copy.16
  6.2 0.7 pad_maximum_fusion.1.kv_in
  6.8 111.0 %layer.1 = bf16[4,64,512]{2,1,0:T(8,128)(2,1)} custom-call(bf16[2,128,1024]{2,1,0:T(8,128)(2,1)} %fusion.2.q_ref, bf16[512,128]{1,0:T(8,128)(2,1)} %pad_maximum_fusion.1.kv_in, bf16[32,2048]{1,0:T(8,128)(2,1)} %up_in.1, bf16[32,2048]{1,0:T(8,128)(2,1)} %bitcast.35, bf16[2,256,2048]{2,1,0:T(8,128)(2,1)} %bitcast.28, bf16[4,64,2048]{2,1,0:T(8,128)(2,1)} %bitcast.31, ...), custom_call_target="tpu_custom_call" | custom-call | tf_op jit(solution)/shard_map/layer/pallas_call | solution.py:556
  117.9 1.7 %copy.21 = bf16[256,512]{1,0:T(8,128)(2,1)} copy(bf16[256,512]{1,0:T(8,128)(2,1)} %bitcast.29) | data formatting | bytes 524288
  (9 shorter events, 0.1 us)
Async XLA Ops:
  2.7 2.3 %copy-start = (bf16[256,128]{1,0:T(8,128)(2,1)S(1)}, bf16[256,128]{1,0:T(8,128)(2,1)}, u32[]{:S(2)}) copy-start(bf16[256,128]{1,0:T(8,128)(2,1)} %param.11) | copy-start | bytes 196612
  2.7 2.6 %copy-start.2 = (f32[64]{0:T(128)S(1)}, f32[64]{0:T(128)}, u32[]{:S(2)}) copy-start(f32[64]{0:T(128)} %param.14) | copy-start | bytes 772
  4.0 2.0 %copy-start.1 = (bf16[256,128]{1,0:T(8,128)(2,1)S(1)}, bf16[256,128]{1,0:T(8,128)(2,1)}, u32[]{:S(2)}) copy-start(bf16[256,128]{1,0:T(8,128)(2,1)} %param.12) | copy-start | bytes 196612

commit v4 on v3

--- a/solution.py
+++ b/solution.py
@@ -15,14 +15,14 @@
 MESH = pl.DeviceIdType.MESH
 
 
-def prepare(projected, gain_vec, offset):
+def prepare(projected, gains, offset):
     row_count = projected.shape[0]
     head_count = projected.shape[1] // HD
     widened = projected.astype(jnp.float32).reshape(row_count, head_count, HD)
     widened = (
         widened
         * lax.rsqrt(jnp.mean(widened * widened, axis=-1, keepdims=True) + EPSILON)
-        * gain_vec
+        * gains
     )
     position = offset + jnp.arange(row_count, dtype=jnp.int32)
     grid_row = (position // GRID_W).astype(jnp.float32)
@@ -345,9 +345,9 @@
     outs = Around(ow_in, ow, 128, at, ow_s, ow_r)
     across = Mail(at, tp_s, tp_r)
 
-    pairs.a(0)
     ups.s1()
     outs.s1()
+    pairs.a(0)
     pairs.a(1)
     pairs.b(0)
     ups.s2()
@@ -355,24 +355,24 @@
     pairs.a(2)
     own[0].wait()
     pairs.c(0)
-    downs.a(0)
+    pairs.w(0)
+    pairs.a(3)
+    pairs.c(1)
     own[1].wait()
     ups.s3()
-    pairs.w(0)
     polls = {
-        1: (lambda: pairs.c(1),),
-        2: (lambda: pairs.w(1),),
-        3: (lambda: pairs.b(2), lambda: pairs.a(3), lambda: downs.a(1),),
-        4: (outs.s2,),
+        1: (lambda: pairs.w(1),),
+        2: (lambda: pairs.b(2),),
+        4: (lambda: pairs.a(4), lambda: pairs.b(3), lambda: downs.a(0), outs.s2,),
         5: (lambda: pairs.c(2),),
-        6: (lambda: pairs.w(2), lambda: ups.z(1),),
-        7: (lambda: pairs.b(3),),
-        8: (lambda: pairs.a(4), lambda: downs.b(0), lambda: downs.a(2),),
-        9: (lambda: pairs.c(3), outs.s3,),
-        10: (lambda: pairs.b(4), lambda: downs.b(1), lambda: ups.z(2), lambda: pairs.w(3),),
-        13: (lambda: downs.a(3), lambda: pairs.c(4),),
+        6: (lambda: downs.a(1), lambda: pairs.b(4), lambda: ups.z(1), lambda: pairs.w(2),),
+        8: (lambda: pairs.c(3),),
+        9: (outs.s3,),
+        10: (lambda: downs.a(2), lambda: pairs.w(3),),
+        12: (lambda: ups.z(2), lambda: pairs.c(4),),
+        13: (lambda: downs.a(3),),
         14: (lambda: pairs.w(4),),
-        15: (lambda: downs.b(2), lambda: ups.z(3),),
+        15: (lambda: downs.b(2),),
     }
 
     def step(n, carry):
@@ -405,15 +405,15 @@
     offsets = (0, -1, 1, 2)
     own[3].wait()
     own[4].wait()
-    outs.w()
     across.send(2, lambda: heads.at[0, at.xat(2)], lambda: heads.at[1, 2], lambda: at.along(2))
     across.send(0, lambda: heads.at[0, at.xat(1)], lambda: heads.at[1, 0], lambda: at.along(1))
     across.send(1, lambda: heads.at[0, at.xat(-1)], lambda: heads.at[1, 1], lambda: at.along(-1))
-    own[2].wait()
-    downs.c(0)
+    outs.w()
+    downs.b(0)
+    downs.b(1)
+    downs.c(2)
+    ups.z(3)
     downs.a(4)
-    downs.b(3)
-    downs.c(1)
     for k in range(3):
         across.got(k, heads.at[1, k])
     lefts = [heads[0, at.x], heads[1, 0], heads[1, 1], heads[1, 2]]
@@ -452,6 +452,8 @@
                 sums = term if sums is None else sums + term
             hid[rows, cols] = jnp.square(jnp.maximum(sums, 0.0)).astype(jnp.bfloat16)
 
+    downs.b(3)
+    ups.z(4)
     norm(0)
     for j in (0, 1):
         chunk = lambda j=j: mid.at[at.xat(-1), j]
@@ -461,29 +463,29 @@
         chunk = lambda j=j: mid.at[at.xat(1), j]
         across.got(7 + j, chunk())
         across.send(11 + j, chunk, chunk, lambda: at.along(-1))
-    downs.b(4)
-    ups.z(4)
-    downs.c(2)
-    ups.w()
-    downs.w(1)
-    downs.w(0)
-    downs.c(4)
-    downs.c(3)
-    lift(0, 1)
     for j in (2, 3):
         across.got(3 + j, mid.at[at.xat(-1), j])
     for j in (0, 1):
         across.got(7 + j, mid.at[at.xat(1), j])
     norm(1)
     norm(2)
-    lift(1, 3)
+    downs.c(1)
+    own[2].wait()
+    downs.c(0)
+    downs.b(4)
+    ups.w()
+    lift(0, 3)
+    downs.c(4)
+    downs.c(3)
     for j in range(4):
         across.got(11 + j, mid.at[at.xat(2), j])
     norm(3)
     lift(3, 4)
+    downs.w(0)
+    downs.w(1)
+    downs.w(4)
+    downs.w(2)
     downs.w(3)
-    downs.w(2)
-    downs.w(4)
 
     def lower(k):
         for t in range(2):

time: 121 us -> 121 us (level)
  no operation moved by 1% of the time
where the time goes in v4:
time: 121 us
  Pallas kernels  112 us (93%)
  local copies, waits for them, and re-layouts  4.45 us (4%)
  other arithmetic  3.84 us (3%)
    pallas_call x1, Pallas kernels, layer(): pl.pallas_call(layer_kernel, name='layer', out_shape=jax.ShapeDtypeStruct...  112 us
    unnamed x10, local copies, waits for them, and re-layouts  2.9 us

profile of v4, /device:TPU:1, one launch (start us, length us, event | category | flops | bytes accessed | tf_op | source)
XLA Modules:
  0.0 120.6 jit_solution(1621519838379640546)
XLA Ops:
  0.0 0.1 broadcast_multiply_fusion.1
  0.1 0.1 fusion.4
  0.2 1.1 copy.12
  1.3 0.3 reshape.157
  1.6 0.1 bitcast_reduce_fusion
  1.7 0.8 mul.172
  2.4 0.3 multiply_multiply_fusion
  2.7 0.0 copy-start
  2.7 0.0 copy-start.2
  2.7 0.7 subtract_convert_fusion
  3.4 0.6 pad_maximum_fusion
  4.0 0.0 copy-start.1
  4.0 0.1 convert_element_type.35
  4.2 0.8 fusion.2.q_ref
  5.1 0.0 copy-done
  5.1 0.1 copy.15
  5.2 0.1 reshape.158
  5.3 0.0 copy-done.2
  5.3 0.1 mul.191
  5.4 0.1 multiply_multiply_fusion.1
  5.5 0.2 subtract_convert_fusion.1
  5.7 0.2 pad_maximum_fusion.2
  5.9 0.1 copy.17
  6.0 0.0 copy-done.1
  6.0 0.1 copy.16
  6.2 0.7 pad_maximum_fusion.1.kv_in
  6.8 112.1 %layer.1 = bf16[4,64,512]{2,1,0:T(8,128)(2,1)} custom-call(bf16[2,128,1024]{2,1,0:T(8,128)(2,1)} %fusion.2.q_ref, bf16[512,128]{1,0:T(8,128)(2,1)} %pad_maximum_fusion.1.kv_in, bf16[32,2048]{1,0:T(8,128)(2,1)} %up_in.1, bf16[32,2048]{1,0:T(8,128)(2,1)} %bitcast.35, bf16[2,256,2048]{2,1,0:T(8,128)(2,1)} %bitcast.28, bf16[4,64,2048]{2,1,0:T(8,128)(2,1)} %bitcast.31, ...), custom_call_target="tpu_custom_call" | custom-call | tf_op jit(solution)/shard_map/layer/pallas_call | solution.py:558
  119.0 1.7 %copy.21 = bf16[256,512]{1,0:T(8,128)(2,1)} copy(bf16[256,512]{1,0:T(8,128)(2,1)} %bitcast.29) | data formatting | bytes 524288
  (9 shorter events, 0.1 us)
Async XLA Ops:
  2.7 2.3 %copy-start = (bf16[256,128]{1,0:T(8,128)(2,1)S(1)}, bf16[256,128]{1,0:T(8,128)(2,1)}, u32[]{:S(2)}) copy-start(bf16[256,128]{1,0:T(8,128)(2,1)} %param.11) | copy-start | bytes 196612
  2.7 2.6 %copy-start.2 = (f32[64]{0:T(128)S(1)}, f32[64]{0:T(128)}, u32[]{:S(2)}) copy-start(f32[64]{0:T(128)} %param.14) | copy-start | bytes 772
  4.0 2.0 %copy-start.1 = (bf16[256,128]{1,0:T(8,128)(2,1)S(1)}, bf16[256,128]{1,0:T(8,128)(2,1)}, u32[]{:S(2)}) copy-start(bf16[256,128]{1,0:T(8,128)(2,1)} %param.12) | copy-start | bytes 196612
